TPU v7x, 32 devices: a whole 2x2x4 slice. The times are simulated.
32 devices in a mesh: sp: 4 (over y, x), tp: 8 (over z, core).
Axes of the slice: x: 2, y: 2, z: 4, core: 2. Of those that a mesh axis runs over, the one named last changes fastest.
Arguments:
- skip_stream_entry: bfloat16 [2048, 2048], P(('sp', 'tp')), may hold values from -6 to 6
- result_switch_mapped: bfloat16 [2048, 4096], P('sp', 'tp'), may hold values from -6 to 6
- channel_feed_mapped: bfloat16 [2048, 4096], P('sp', 'tp'), may hold values from -6 to 6
- write_coefficient_mapped: bfloat16 [2048, 2048], P('sp', 'tp'), may hold values from -6 to 6
- emission_coefficient_mapped: bfloat16 [2048, 2048], P('sp', 'tp'), may hold values from -6 to 6
- channel_feed_taps: bfloat16 [5, 4096], P(None, 'tp'), may hold values from -2.5 to 2.5
- write_coefficient_taps: bfloat16 [5, 2048], P(None, 'tp'), may hold values from -2.5 to 2.5
- emission_coefficient_taps: bfloat16 [5, 2048], P(None, 'tp'), may hold values from -2.5 to 2.5
- raw_increments: bfloat16 [2, 64, 2048], P(None, 'tp', 'sp'), may hold values from -6 to 6
- channel_log_fade_speed: float32 [2, 64], P(None, 'tp'), may hold values from -20 to 0
- extra_log_fade: float32 [2, 64, 2048], P(None, 'tp', 'sp'), may hold values from -1 to 0
- cluster_scaling_factor: float32 [4096], P('tp'), may hold values from 0.1 to 1.9
- blend_result_matrix: bfloat16 [4096, 2048], P('tp'), may hold values from -0.09375 to 0.09375
- routing_scaling_factor: float32 [2048], replicated, may hold values from 0.1 to 1.9
- specialist_switch_matrix: bfloat16 [8, 2048, 4096], P('sp', None, 'tp'), may hold values from -0.125 to 0.125
- specialist_widen_matrix: bfloat16 [8, 2048, 4096], P('sp', None, 'tp'), may hold values from -0.125 to 0.125
- specialist_contract_matrix: bfloat16 [8, 4096, 2048], P('sp', 'tp'), may hold values from -0.1875 to 0.1875
- picked_specialists: int32 [2048, 2], P(('sp', 'tp')), may hold values from 0 to 7, all different within a row; in each aligned block of 64 rows (0 to 63, 64 to 127, ...) at most 24 rows name the same one
- router_affinities: float32 [2048, 2], P(('sp', 'tp')), may hold values from 0.1 to 1
Outputs:
- result: bfloat16 [2048, 2048], P(('sp', 'tp'))
Inputs may be any that keep to these rules, and one draw needn't show every extreme that they name: `picked_specialists`: each row names 2 different experts. Within the rows of one device (aligned blocks of 64 rows) no expert is named more than 24 times, a bound that some block reaches.
All inputs are finite; a program needn't handle non-finite values.
Results may differ from a plain program's by a relative error of at most 0.02.
Values may be sent and summed in bfloat16 or wider, within the bound.
No kernel may reach another device: no remote copies, remote signals or barrier semaphores. Data moves between devices by JAX's collectives and lax.ppermute only.
A program may use at most 64 MiB of HBM per device.

v0:
```python
import functools
import math

import jax
import jax.numpy as jnp
from jax import lax
from jax.experimental import pallas as pl
from jax.experimental.pallas import tpu as pltpu
from jax.sharding import PartitionSpec as P


HEAD_DIM = 64
STATE = 128
TOP = 2
TILE = 128
PAD = 8
EXTRA = 16

EPSILON = 1e-06
LOG2E = math.log2(math.e)
F32, BF16 = jnp.float32, jnp.bfloat16


CORES = 2
CHUNKS = 2


def chip_and_core(axis):
    at = lax.axis_index(axis)
    return at // CORES, at & (CORES - 1)


def silu(v):
    return v / (1.0 + jnp.exp(-v))


def over_heads(columns, first, count):
    rows = columns.shape[0]
    lane = lax.broadcasted_iota(jnp.int32, (rows, 2 * HEAD_DIM), 1)
    pairs = []
    for h in range(0, count, 2):
        a = jnp.broadcast_to(columns[:, first + h : first + h + 1], lane.shape)
        b = jnp.broadcast_to(columns[:, first + h + 1 : first + h + 2], lane.shape)
        pairs.append(jnp.where(lane < HEAD_DIM, a, b))
    return jnp.concatenate(pairs, axis=1)


def route_kernel(picked_ref, affinity_ref, meta_ref, *, room):
    rows = picked_ref.shape[0]
    lane = lax.broadcasted_iota(jnp.int32, (rows, TILE), 1)
    picks = [jnp.broadcast_to(picked_ref[:, k : k + 1], (rows, TILE)) == lane for k in range(TOP)]
    member = jnp.where(picks[0] | picks[1], 1.0, 0.0)
    earlier = lax.broadcasted_iota(jnp.int32, (rows, rows), 0) > lax.broadcasted_iota(
        jnp.int32, (rows, rows), 1
    )
    rank = jnp.dot(
        jnp.where(earlier, 1.0, 0.0).astype(BF16), member.astype(BF16), preferred_element_type=F32
    )
    affinity = affinity_ref[...]
    total = jnp.sum(affinity, axis=1, keepdims=True)
    meta = jnp.zeros((rows, TILE), F32)
    for k in range(TOP):
        slot = picked_ref[:, k : k + 1].astype(F32) * room + jnp.sum(
            jnp.where(picks[k], rank, 0.0), axis=1, keepdims=True
        )
        meta = jnp.where(lane == k, slot, meta)
        meta = jnp.where(lane == TOP + k, affinity[:, k : k + 1] / total, meta)
    meta_ref[...] = meta


def early_kernel(
    raw_ref, speed_ref, fade_ref, rows_ref, cols_ref, totals_ref
):
    heads, steps = raw_ref.shape[1:]
    lane = lax.broadcasted_iota(jnp.int32, (heads, steps), 1)
    eye = lax.broadcasted_iota(jnp.int32, (heads, heads), 0) == lax.broadcasted_iota(
        jnp.int32, (heads, heads), 1
    )
    sums, weights = [], []
    for d in range(2):
        raw = raw_ref[d].astype(F32)
        step = jnp.maximum(raw, 0.0) + jnp.log1p(jnp.exp(-jnp.abs(raw)))
        speed = jnp.sum(
            jnp.where(eye, jnp.exp(speed_ref[d : d + 1, :]), 0.0), axis=1, keepdims=True
        )
        run = -step * speed + fade_ref[d]
        shift = 1
        while shift < steps:
            if d == 0:
                run = run + jnp.where(lane >= shift, pltpu.roll(run, shift, 1), 0.0)
            else:
                run = run + jnp.where(lane < steps - shift, pltpu.roll(run, steps - shift, 1), 0.0)
            shift *= 2
        total = run[:, steps - 1 : steps] if d == 0 else run[:, 0:1]
        totals_ref[d] = jnp.broadcast_to(total, (heads, STATE))
        sums.append(run * LOG2E)
        weights.append(jnp.exp(total - run) * step)
        rows_ref[d] = run * LOG2E - jnp.log(step) * LOG2E
    stacked = jnp.concatenate(
        sums + weights + [jnp.zeros((STATE - 4 * heads, steps), F32)], axis=0
    )
    cols_ref[...] = stacked.T


def prepare_kernel(
    x_ref, b_ref, c_ref, low_ref, high_ref, tx_ref, tb_ref, tc_ref, cols_ref, totals_ref,
    xc_ref, bc_ref, cc_ref, *rest, axis,
):
    *msg_refs, pad_ref = rest
    steps = x_ref.shape[0]
    heads = totals_ref.shape[1]
    groups = b_ref.shape[1] // STATE
    per_group = heads // groups
    wide = per_group * HEAD_DIM
    here = lax.axis_index(axis)
    cols = cols_ref[...]
    totals = [totals_ref[d, :, 0:1] for d in range(2)]

    def conv(ref, taps_ref, at, start):
        pad_ref[PAD - 2 : PAD] = low_ref[:, at + start : at + start + TILE].astype(F32)
        pad_ref[PAD : PAD + steps] = ref[:, start : start + TILE].astype(F32)
        pad_ref[PAD + steps : PAD + steps + 2] = high_ref[
            :, at + start : at + start + TILE
        ].astype(F32)
        taps = taps_ref[:, start : start + TILE].astype(F32)
        total = taps[0:1] * pad_ref[PAD - 2 : PAD - 2 + steps]
        for j in range(1, taps.shape[0]):
            total = total + taps[j : j + 1] * pad_ref[PAD - 2 + j : PAD - 2 + j + steps]
        return silu(total)

    at = 0
    for ref, taps_ref, out_ref in (
        (x_ref, tx_ref, xc_ref), (b_ref, tb_ref, bc_ref), (c_ref, tc_ref, cc_ref),
    ):
        for start in range(0, ref.shape[1], TILE):
            out_ref[:, start : start + TILE] = conv(ref, taps_ref, at, start).astype(BF16)
        at += ref.shape[1]

    row = lax.broadcasted_iota(jnp.int32, (EXTRA, wide), 0)
    own = lax.broadcasted_iota(jnp.int32, (per_group, wide), 0) == (
        lax.broadcasted_iota(jnp.int32, (per_group, wide), 1) // HEAD_DIM
    )
    for g in range(groups):
        turned = bc_ref[:, g * STATE : (g + 1) * STATE].astype(F32).T.astype(BF16)
        xg = xc_ref[:, g * wide : (g + 1) * wide].astype(F32)
        both = []
        for d in range(2):
            weight = over_heads(cols, (2 + d) * heads + g * per_group, per_group)
            state = jnp.dot(turned, (xg * weight).astype(BF16), preferred_element_type=F32)
            total = jnp.sum(
                jnp.where(own, totals[d][g * per_group : (g + 1) * per_group], 0.0),
                axis=0, keepdims=True,
            )
            upper = total.astype(BF16).astype(F32)
            extra = jnp.where(row == 0, upper, jnp.where(row == 1, total - upper, 0.0))
            both.append((state, extra))
        for k, msg_ref in enumerate(msg_refs, 1):
            onward = jnp.where((here ^ k) > here, 1.0, 0.0).astype(F32)
            (sf, ef), (sb, eb) = both
            msg_ref[g, 0:STATE, :] = (sf * onward + sb * (1.0 - onward)).astype(BF16)
            msg_ref[g, STATE : STATE + EXTRA, :] = (ef * onward + eb * (1.0 - onward)).astype(BF16)


def local_kernel(xc_ref, bc_ref, cc_ref, rows_ref, cols_ref, y_ref):
    steps = xc_ref.shape[0]
    heads = rows_ref.shape[1]
    groups = bc_ref.shape[1] // STATE
    per_group = heads // groups
    tiles = steps // TILE
    i_at = lax.broadcasted_iota(jnp.int32, (TILE, TILE), 0)
    j_at = lax.broadcasted_iota(jnp.int32, (TILE, TILE), 1)
    for g in range(groups):
        for i in range(tiles):
            span = slice(i * TILE, (i + 1) * TILE)
            inner = lax.dot_general(
                cc_ref[span, g * STATE : (g + 1) * STATE],
                bc_ref[:, g * STATE : (g + 1) * STATE],
                (((1,), (1,)), ((), ())),
                preferred_element_type=F32,
            )
            for pair in range(per_group // 2):
                halves = []
                at = (g * per_group + 2 * pair) * HEAD_DIM
                for h in (g * per_group + 2 * pair, g * per_group + 2 * pair + 1):
                    here_f = jnp.broadcast_to(cols_ref[span, h : h + 1], (TILE, TILE))
                    here_b = jnp.broadcast_to(cols_ref[span, heads + h : heads + h + 1], (TILE, TILE))
                    parts = []
                    for j in range(tiles):
                        js = slice(j * TILE, (j + 1) * TILE)
                        if j <= i:
                            mix = jnp.exp2(here_f - rows_ref[0, h : h + 1, js])
                            if j == i:
                                mix = jnp.where(i_at >= j_at, mix, 0.0) + jnp.where(
                                    i_at <= j_at, jnp.exp2(here_b - rows_ref[1, h : h + 1, js]), 0.0
                                )
                        else:
                            mix = jnp.exp2(here_b - rows_ref[1, h : h + 1, js])
                        parts.append((mix * inner[:, js]).astype(BF16))
                    halves.append(
                        jnp.dot(
                            jnp.concatenate(parts, axis=1),
                            xc_ref[:, at : at + 2 * HEAD_DIM],
                            preferred_element_type=F32,
                        )
                    )
                y_ref[span, at : at + 2 * HEAD_DIM] = jnp.where(j_at < HEAD_DIM, *halves)


def finish_kernel(y_ref, cc_ref, cols_ref, switch_ref, gain_ref, *rest, axis, minor, rows):
    *msg_refs, keep_ref, send_ref, carry_ref = rest
    steps, channels = y_ref.shape
    groups = cc_ref.shape[1] // STATE
    wide = channels // groups
    per_group = wide // HEAD_DIM
    heads = groups * per_group
    here = lax.axis_index(axis)
    chip, core = chip_and_core(minor)
    chips = lax.axis_size(minor) // CORES
    peers = [here ^ k for k in range(1, len(msg_refs) + 1)]

    def flag(condition):
        return jnp.where(condition, 1.0, 0.0).astype(F32)

    for g in range(groups):
        totals = [
            ref[g, STATE : STATE + 1, :].astype(F32) + ref[g, STATE + 1 : STATE + 2, :].astype(F32)
            for ref in msg_refs
        ]
        for d in range(2):
            carry = jnp.zeros((STATE, wide), F32)
            for k, ref in enumerate(msg_refs):
                between = jnp.zeros((1, wide), F32)
                for other in range(len(msg_refs)):
                    if other != k:
                        if d == 0:
                            inside = (peers[k] < peers[other]) & (peers[other] < here)
                        else:
                            inside = (peers[k] > peers[other]) & (peers[other] > here)
                        between = between + flag(inside) * totals[other]
                mine = flag(peers[k] < here if d == 0 else peers[k] > here)
                carry = carry + ref[g, 0:STATE, :].astype(F32) * (mine * jnp.exp(between))
            carry_ref[d] = carry.astype(BF16)
        for i in range(steps // TILE):
            span = slice(i * TILE, (i + 1) * TILE)
            lanes = slice(g * wide, (g + 1) * wide)
            cols = jnp.exp2(cols_ref[span, :])
            cc = cc_ref[span, g * STATE : (g + 1) * STATE]
            y = y_ref[span, lanes]
            for d in range(2):
                y = y + over_heads(cols, d * heads + g * per_group, per_group) * jnp.dot(
                    cc, carry_ref[d], preferred_element_type=F32
                )
            gated = y * silu(switch_ref[span, lanes].astype(F32))
            mean = jnp.sum(gated * gated, axis=1, keepdims=True) * (1.0 / wide)
            mixed = gated * lax.rsqrt(mean + EPSILON) * gain_ref[:, lanes]
            for part in range(TILE // (CORES * rows)):
                block = i * (TILE // (CORES * rows)) + part
                south = mixed[part * CORES * rows : (part * CORES + 1) * rows]
                north = mixed[(part * CORES + 1) * rows : (part + 1) * CORES * rows]
                odd = flag(core == 1)
                at = pl.multiple_of(((block - chip) & (chips - 1)) * rows, rows)
                keep_ref[pl.ds(at, rows), lanes] = (south * (1.0 - odd) + north * odd).astype(BF16)
                send_ref[pl.ds(at, rows), lanes] = (south * odd + north * (1.0 - odd)).astype(BF16)


def kernel(body, operands, outs, grant=12, **settings):
    return pl.pallas_call(
        body,
        out_shape=outs,
        out_specs=vmem(len(outs)) if isinstance(outs, list) else vmem(1)[0],
        compiler_params=pltpu.CompilerParams(vmem_limit_bytes=grant * 1024 * 1024),
        **{"in_specs": vmem(len(operands)), **settings},
    )(*operands)


def vmem(count):
    return [pl.BlockSpec(memory_space=pltpu.VMEM) for _ in range(count)]


def mixer(x, b, c, tx, tb, tc, early, switch, gain, block_rows):
    steps, channels = x.shape
    groups = b.shape[1] // STATE
    wide = channels // groups
    rim = tx.shape[0] // 2
    count = lax.axis_size("sp")
    first = jnp.concatenate([x[:rim], b[:rim], c[:rim]], axis=1)
    last = jnp.concatenate([x[-rim:], b[-rim:], c[-rim:]], axis=1)
    low = lax.ppermute(last, "sp", [(i, i + 1) for i in range(count - 1)])
    high = lax.ppermute(first, "sp", [(i + 1, i) for i in range(count - 1)])
    rows, cols, totals = early()
    heads = rows.shape[1]
    message = jax.ShapeDtypeStruct((groups, STATE + EXTRA, wide), BF16)
    xc, bc, cc, *sends = kernel(
        functools.partial(prepare_kernel, axis="sp"),
        (x, b, c, low, high, tx, tb, tc, cols, totals),
        [jax.ShapeDtypeStruct(v.shape, BF16) for v in (x, b, c)] + [message] * (count - 1),
        scratch_shapes=[pltpu.VMEM((steps + 2 * PAD, TILE), F32)],
    )
    arrived = [
        lax.ppermute(send, "sp", [(i, i ^ k) for i in range(count)])
        for k, send in enumerate(sends, 1)
    ]
    y = kernel(
        local_kernel,
        (xc, bc, cc, rows, cols),
        jax.ShapeDtypeStruct(x.shape, F32),
        cost_estimate=pl.CostEstimate(
            flops=2 * steps * steps * (channels + groups * STATE) * 4,
            bytes_accessed=8 * steps * channels,
            transcendentals=heads * steps * steps,
        ),
    )
    return kernel(
        functools.partial(finish_kernel, axis="sp", minor="tp", rows=block_rows),
        (y, cc, cols, switch, gain.reshape(1, -1), *arrived),
        [jax.ShapeDtypeStruct((steps // CORES, channels), BF16)] * 2,
        scratch_shapes=[pltpu.VMEM((2, STATE, wide), BF16)],
    )


def project_kernel(keep_ref, other_ref, own_w_ref, other_w_ref, *out_refs):
    rows = out_refs[0].shape[0]
    width = own_w_ref.shape[1]
    step = 2 * TILE
    for n in range(0, width, step):
        lanes = slice(n, n + step)
        part = jnp.dot(keep_ref[...], own_w_ref[:, lanes], preferred_element_type=F32) + jnp.dot(
            other_ref[...], other_w_ref[:, lanes], preferred_element_type=F32
        )
        for r, out_ref in enumerate(out_refs):
            out_ref[:, lanes] = part[r * rows : (r + 1) * rows].astype(BF16)


def after_kernel(skip_ref, gain_ref, *refs, chips):
    part_refs, (after_ref, *normed_refs) = refs[:chips], refs[chips:]
    total = skip_ref[...].astype(F32)
    for ref in part_refs:
        total = total + ref[...].astype(F32)
    after = total.astype(BF16)
    after_ref[...] = after
    values = after.astype(F32)
    mean = jnp.sum(values * values, axis=1, keepdims=True) * (1.0 / values.shape[1])
    normed = (values * lax.rsqrt(mean + EPSILON) * gain_ref[...]).astype(BF16)
    step = normed_refs[0].shape[1]
    for n, ref in enumerate(normed_refs):
        ref[...] = normed[:, n * step : (n + 1) * step]


def final_kernel(after_ref, *refs, chunks):
    *in_refs, out_ref = refs
    each = len(in_refs) // chunks
    for n in range(chunks):
        step = in_refs[0].shape[1]
        lanes = slice(n * step, (n + 1) * step)
        total = after_ref[:, lanes].astype(F32)
        for ref in in_refs[n * each : (n + 1) * each]:
            total = total + ref[...].astype(F32)
        out_ref[:, lanes] = total.astype(BF16)


def dispatch_kernel(*refs, chips, room, axis, minor):
    meta_refs, x_refs, out_refs = refs[:chips], refs[chips : 2 * chips], refs[2 * chips :]
    rows, width = x_refs[0].shape
    here = lax.axis_index(axis)
    core = chip_and_core(minor)[1]
    meta = jnp.concatenate([ref[...] for ref in meta_refs], axis=0).T
    rank = lax.broadcasted_iota(jnp.int32, (room, chips * rows), 0).astype(F32)
    source = lax.broadcasted_iota(jnp.int32, (room, chips * rows), 1) // rows
    chosen = []
    for o in range(len(out_refs)):
        expert = (here ^ (o // CORES)) * CORES + (core ^ (o % CORES))
        first = (expert * room).astype(F32)
        hit = (meta[0:1] - first == rank) | (meta[1:2] - first == rank)
        chosen += [
            jnp.where(hit & (source == r), 1.0, 0.0).astype(F32) for r in range(chips)
        ]
    chosen = jnp.concatenate(chosen, axis=0).astype(BF16)
    for n in range(0, width, 2 * TILE):
        lanes = slice(n, n + 2 * TILE)
        tokens = jnp.concatenate([ref[:, lanes] for ref in x_refs], axis=0)
        out = jnp.dot(chosen, tokens, preferred_element_type=F32).astype(BF16)
        for o, ref in enumerate(out_refs):
            ref[:, lanes] = out[o * chips * room : (o + 1) * chips * room]


def combine_kernel(*refs, chips, room, axis, minor):
    meta_refs, in_refs, out_refs = refs[:chips], refs[chips:-chips], refs[-chips:]
    rows, width = out_refs[0].shape
    here = lax.axis_index(axis)
    core = chip_and_core(minor)[1]
    lane = lax.broadcasted_iota(jnp.int32, (rows, chips * room), 1)
    weights = []
    for r in range(chips):
        meta = meta_refs[r][...]
        parts = []
        for o in range(len(in_refs)):
            expert = (here ^ (o // CORES)) * CORES + (core ^ (o % CORES))
            slot = (lane - r * room + expert * room).astype(F32)
            inside = (lane >= r * room) & (lane < (r + 1) * room)
            both = jnp.where(meta[:, 0:1] == slot, meta[:, TOP : TOP + 1], 0.0) + jnp.where(
                meta[:, 1:2] == slot, meta[:, TOP + 1 : TOP + 2], 0.0
            )
            parts.append(jnp.where(inside, both, 0.0).astype(BF16))
        weights.append(parts)
    for n in range(0, width, 2 * TILE):
        lanes = slice(n, n + 2 * TILE)
        total = jnp.zeros((chips * rows, 2 * TILE), F32)
        for o, ref in enumerate(in_refs):
            weight = jnp.concatenate([weights[r][o] for r in range(chips)], axis=0)
            total = total + jnp.dot(weight, ref[:, lanes], preferred_element_type=F32)
        for r, ref in enumerate(out_refs):
            ref[:, lanes] = total[r * rows : (r + 1) * rows].astype(BF16)


def hidden_kernel(*refs, count, chunks, minor):
    x_refs, weight_refs, refs = refs[:count], refs[count : count + 4], refs[count + 4 :]
    hidden_ref, x_vmem, gate_vmem, up_vmem, sems = refs
    core = chip_and_core(minor)[1]
    slabs, _, step = gate_vmem.shape
    per_source = slabs // 2
    copies = []
    for t in range(slabs):
        gate, up = weight_refs[0:2] if t < per_source else weight_refs[2:4]
        span = pl.ds((t % per_source) * step, step)
        copies.append(
            [
                pltpu.make_async_copy(gate.at[core, :, span], gate_vmem.at[t], sems.at[t, 0]),
                pltpu.make_async_copy(up.at[core, :, span], up_vmem.at[t], sems.at[t, 1]),
            ]
        )
    for group in copies:
        for copy in group:
            copy.start()
    rows, columns = x_refs[0].shape
    for o, ref in enumerate(x_refs):
        at, n = o // chunks * rows, o % chunks * columns
        x_vmem[at : at + rows, n : n + columns] = ref[...]
    for t in range(slabs):
        for copy in copies[t]:
            copy.wait()
        gate = jnp.dot(x_vmem[...], gate_vmem[t], preferred_element_type=F32)
        up = jnp.dot(x_vmem[...], up_vmem[t], preferred_element_type=F32)
        hidden_ref[:, t * step : (t + 1) * step] = (silu(gate) * up).astype(BF16)


def down_kernel(hidden_ref, own_ref, other_ref, *refs, chunk, minor):
    *out_refs, down_vmem, sems = refs
    core = chip_and_core(minor)[1]
    rows, columns = out_refs[0].shape
    half, step = down_vmem.shape[0] // 2, 2 * TILE
    copies = []
    for n in range(0, columns, step):
        for side, ref in enumerate((own_ref, other_ref)):
            copies.append(
                pltpu.make_async_copy(
                    ref.at[core, :, pl.ds(chunk * columns + n, step)],
                    down_vmem.at[pl.ds(side * half, half), pl.ds(n, step)],
                    sems.at[n // step, side],
                )
            )
    for copy in copies:
        copy.start()
    for n in range(0, columns, step):
        copies[n // step * 2].wait()
        copies[n // step * 2 + 1].wait()
        part = jnp.dot(
            hidden_ref[...], down_vmem[:, n : n + step], preferred_element_type=F32
        ).astype(BF16)
        for o, ref in enumerate(out_refs):
            ref[:, n : n + step] = part[o * rows : (o + 1) * rows]


def run_experts(messages, own, other, chunks):
    flat = [part for message in messages for part in message]
    rows, columns = flat[0].shape
    total_rows, width = len(messages) * rows, columns * chunks
    hidden = own[0].shape[2]
    step = 2 * TILE if hidden % (2 * TILE) == 0 else hidden
    slabs = 2 * (hidden // step)
    inner = kernel(
        functools.partial(hidden_kernel, count=len(flat), chunks=chunks, minor="tp"),
        (*flat, own[0], own[1], other[0], other[1]),
        jax.ShapeDtypeStruct((total_rows, 2 * hidden), BF16),
        grant=28,
        in_specs=vmem(len(flat)) + [pl.BlockSpec(memory_space=pltpu.HBM)] * 4,
        scratch_shapes=[
            pltpu.VMEM((total_rows, width), BF16),
            pltpu.VMEM((slabs, width, step), BF16),
            pltpu.VMEM((slabs, width, step), BF16),
            pltpu.SemaphoreType.DMA((slabs, 2)),
        ],
        cost_estimate=pl.CostEstimate(
            flops=8 * total_rows * width * hidden,
            bytes_accessed=8 * hidden * width,
            transcendentals=total_rows * 2 * hidden,
        ),
    )
    return [
        kernel(
            functools.partial(down_kernel, chunk=n, minor="tp"),
            (inner, own[2], other[2]),
            [jax.ShapeDtypeStruct((rows, columns), BF16)] * len(messages),
            in_specs=vmem(1) + [pl.BlockSpec(memory_space=pltpu.HBM)] * 2,
            scratch_shapes=[
                pltpu.VMEM((2 * hidden, columns), BF16),
                pltpu.SemaphoreType.DMA((columns // (2 * TILE), 2)),
            ],
            cost_estimate=pl.CostEstimate(
                flops=4 * total_rows * columns * hidden,
                bytes_accessed=4 * hidden * columns,
                transcendentals=0,
            ),
        )
        for n in range(chunks)
    ]


def per_device(
    skip_stream_entry,
    result_switch_mapped,
    channel_feed_mapped,
    write_coefficient_mapped,
    emission_coefficient_mapped,
    channel_feed_taps,
    write_coefficient_taps,
    emission_coefficient_taps,
    raw_increments,
    channel_log_fade_speed,
    extra_log_fade,
    cluster_scaling_factor,
    blend_result_matrix,
    routing_scaling_factor,
    specialist_switch_matrix,
    specialist_widen_matrix,
    specialist_contract_matrix,
    picked_specialists,
    router_affinities,
):
    rows, width = skip_stream_entry.shape
    peers, minor = lax.axis_size("sp"), lax.axis_size("tp")
    chips = minor // CORES
    assert specialist_switch_matrix.shape[0] == CORES
    experts = CORES * peers
    capacity = max(2, 3 * TOP * rows // (2 * experts))
    room = -(-capacity // 8) * 8

    def to_partner(value):
        return lax.ppermute(value, "tp", [(t, t ^ 1) for t in range(minor)])

    def to_chip(value, ahead):
        pairs = [(t, (t + CORES * ahead) % minor) for t in range(minor)]
        return lax.ppermute(value, "tp", pairs)

    def to_peer(value, o):
        pairs = [
            (s * minor + t, (s ^ (o // CORES)) * minor + (t ^ (o % CORES)))
            for s in range(peers)
            for t in range(minor)
        ]
        return lax.ppermute(value, ("sp", "tp"), pairs)

    piece = jax.ShapeDtypeStruct((rows, width), BF16)
    slim = jax.ShapeDtypeStruct((rows, width // CHUNKS), BF16)
    message = jax.ShapeDtypeStruct((chips * room, width // CHUNKS), BF16)

    def early():
        return kernel(
            early_kernel,
            (raw_increments, channel_log_fade_speed, extra_log_fade),
            [
                jax.ShapeDtypeStruct(raw_increments.shape, F32),
                jax.ShapeDtypeStruct((raw_increments.shape[2], STATE), F32),
                jax.ShapeDtypeStruct((*raw_increments.shape[:2], STATE), F32),
            ],
        )

    keep, send = mixer(
        channel_feed_mapped,
        write_coefficient_mapped,
        emission_coefficient_mapped,
        channel_feed_taps,
        write_coefficient_taps,
        emission_coefficient_taps,
        early,
        result_switch_mapped,
        cluster_scaling_factor,
        rows,
    )
    own = (specialist_switch_matrix, specialist_widen_matrix, specialist_contract_matrix)
    other = tuple(to_partner(value) for value in own)
    parts = kernel(
        project_kernel,
        (keep, to_partner(send), blend_result_matrix, to_partner(blend_result_matrix)),
        [piece] * chips,
    )
    parts = [parts[0]] + [to_chip(parts[r], r) for r in range(1, chips)]
    after, *normed = kernel(
        functools.partial(after_kernel, chips=chips),
        (skip_stream_entry, routing_scaling_factor.reshape(1, -1), *parts),
        [piece] + [slim] * CHUNKS,
    )
    meta = kernel(
        functools.partial(route_kernel, room=room),
        (picked_specialists, router_affinities),
        jax.ShapeDtypeStruct((rows, TILE), F32),
    )
    metas = [meta] + [to_chip(meta, r) for r in range(1, chips)]
    places = dict(chips=chips, room=room, axis="sp", minor="tp")
    messages = []
    for n in range(CHUNKS):
        tokens = [normed[n]] + [to_chip(normed[n], r) for r in range(1, chips)]
        sends = kernel(
            functools.partial(dispatch_kernel, **places), (*metas, *tokens), [message] * experts
        )
        messages.append([sends[0]] + [to_peer(sends[o], o) for o in range(1, experts)])
    bounds = group_bounds(peers)
    results = [[] for _ in range(CHUNKS)]
    for first, last in zip(bounds[:-1], bounds[1:]):
        part = [[messages[n][o] for n in range(CHUNKS)] for o in range(first, last)]
        done = run_experts(part, own, other, CHUNKS)
        for n in range(CHUNKS):
            results[n] += done[n]
    pieces = []
    for n in range(CHUNKS):
        back = [results[n][0]] + [to_peer(results[n][o], o) for o in range(1, experts)]
        sums = kernel(functools.partial(combine_kernel, **places), (*metas, *back), [slim] * chips)
        pieces += [sums[0]] + [to_chip(sums[chips - r], r) for r in range(1, chips)]
    return kernel(functools.partial(final_kernel, chunks=CHUNKS), (after, *pieces), piece)


def group_bounds(peers):
    return [0, CORES, CORES * peers]


def solution(mesh):
    in_specs = (
        P(("sp", "tp"), None),
        P("sp", "tp"),
        P("sp", "tp"),
        P("sp", "tp"),
        P("sp", "tp"),
        P(None, "tp"),
        P(None, "tp"),
        P(None, "tp"),
        P(None, "tp", "sp"),
        P(None, "tp"),
        P(None, "tp", "sp"),
        P("tp"),
        P("tp", None),
        P(),
        P("sp", None, "tp"),
        P("sp", None, "tp"),
        P("sp", "tp", None),
        P(("sp", "tp"), None),
        P(("sp", "tp"), None),
    )
    out_specs = P(("sp", "tp"), None)

    return jax.shard_map(
        per_device, mesh=mesh, in_specs=in_specs, out_specs=out_specs, check_vma=False
    )
```

profile of v0, /device:TPU:0, one launch (start us, length us, event | category | flops | bytes accessed | tf_op | source)
XLA Modules:
  0.0 234.3 jit_solution(10807158013294407996)
XLA Ops:
  2.5 4.8 %collective-permute-start = (bf16[2,1024]{1,0:T(2,128)(2,1)S(1)}, bf16[2,1024]{1,0:T(2,128)(2,1)S(1)}, u32[]{:S(2)}, u32[]{:S(2)}) collective-permute-start(bf16[2,1024]{1,0:T(2,128)(2,1)S(1)} %pad_maximum_fusion), channel_id=1, source_target_pairs={{0,8},{8,16},{16,24},{1,9},{9,17},{17,25},{2,10},{10,18},{18,26},{... | collective-permute-start | bytes 12296 | tf_op jit(solution)/shard_map/ppermute | solution.py:288
  19.5 3.1 %shard_map.182 = (bf16[512,512]{1,0:T(8,128)(2,1)S(1)}, bf16[512,256]{1,0:T(8,128)(2,1)S(1)}, bf16[512,256]{1,0:T(8,128)(2,1)S(1)}, bf16[2,144,256]{2,1,0:T(8,12...) custom-call(bf16[512,512]{1,0:T(8,128)(2,1)S(1)} %copy-done.6, ...), custom_call_target="tpu_custom_call" | custom-call | tf_op jit(solution)/shard_map/pallas_call | solution.py:267
  25.6 3.1 %collective-permute-done.2.rest_0_ = bf16[2,144,256]{2,1,0:T(8,128)(2,1)S(1)} collective-permute-done((bf16[2,144,256]{2,1,0:T(8,128)(2,1)S(1)}, bf16[2,144,256]{2,1,0:T(8,128)(2,1)S(1)}, u32[]{:S(2)}, u32[]{:S(2)}) %collective-permute-start.2) | collective-permute-done | bytes 147488 | tf_op jit(solution)/shard_map/ppermute | solution.py:300
  33.9 4.5 %collective-permute-start.4 = (bf16[2,144,256]{2,1,0:T(8,128)(2,1)S(1)}, bf16[2,144,256]{2,1,0:T(8,128)(2,1)S(1)}, u32[]{:S(2)}, u32[]{:S(2)}) collective-permute-start(bf16[2,144,256]{2,1,0:T(8,128)(2,1)S(1)} %get-tuple-element.71), channel_id=1, source_target_pairs={{0,24},{8,16},{16,8},{24,0},{1,25},{9,17},{17,9},{25,1},{2,26},{10... | collective-permute-start | bytes 442376 | tf_op jit(solution)/shard_map/ppermute | solution.py:300
  50.7 6.9 %collective-permute-done.7.refs_1_ = bf16[64,2048]{1,0:T(8,128)(2,1)S(1)} collective-permute-done((bf16[64,2048]{1,0:T(8,128)(2,1)S(1)}, bf16[64,2048]{1,0:T(8,128)(2,1)S(1)}, u32[]{:S(2)}, u32[]{:S(2)}) %collective-permute-start.7) | collective-permute-done | bytes 262176 | tf_op jit(solution)/shard_map/ppermute | solution.py:552
  59.3 8.7 %collective-permute-done.8.refs_2_ = bf16[64,2048]{1,0:T(8,128)(2,1)S(1)} collective-permute-done((bf16[64,2048]{1,0:T(8,128)(2,1)S(1)}, bf16[64,2048]{1,0:T(8,128)(2,1)S(1)}, u32[]{:S(2)}, u32[]{:S(2)}) %collective-permute-start.8) | collective-permute-done | bytes 262176 | tf_op jit(solution)/shard_map/ppermute | solution.py:552
  68.1 7.2 %collective-permute-start.12 = (f32[64,128]{1,0:T(8,128)S(1)}, f32[64,128]{1,0:T(8,128)S(1)}, u32[]{:S(2)}, u32[]{:S(2)}) collective-permute-start(f32[64,128]{1,0:T(8,128)S(1)} %shard_map.187.refs_0_), channel_id=1, source_target_pairs={{0,6},{1,7},{2,0},{3,1},{4,2},{5,3},{6,4},{7,5},{8,14},{9,15},{10,... | collective-permute-start | bytes 98312 | tf_op jit(solution)/shard_map/ppermute | solution.py:552
  76.8 4.1 %collective-permute-start.18 = (bf16[64,1024]{1,0:T(8,128)(2,1)S(1)}, bf16[64,1024]{1,0:T(8,128)(2,1)S(1)}, u32[]{:S(2)}, u32[]{:S(2)}) collective-permute-start(bf16[64,1024]{1,0:T(8,128)(2,1)S(1)} %get-tuple-element.81.refs_4_), channel_id=1, source_target_pairs={{0,6},{1,7},{2,0},{3,1},{4,2},{5,3},{6,4},{7,5},{8,14},{9,15},{10,... | collective-permute-start | bytes 393224 | tf_op jit(solution)/shard_map/ppermute | solution.py:552
  80.9 6.1 %collective-permute-done.10.refs_1_ = f32[64,128]{1,0:T(8,128)S(1)} collective-permute-done((f32[64,128]{1,0:T(8,128)S(1)}, f32[64,128]{1,0:T(8,128)S(1)}, u32[]{:S(2)}, u32[]{:S(2)}) %collective-permute-start.10) | collective-permute-done | bytes 32800 | tf_op jit(solution)/shard_map/ppermute | solution.py:552
  87.1 8.8 %collective-permute-done.17.refs_6_ = bf16[64,1024]{1,0:T(8,128)(2,1)S(1)} collective-permute-done((bf16[64,1024]{1,0:T(8,128)(2,1)S(1)}, bf16[64,1024]{1,0:T(8,128)(2,1)S(1)}, u32[]{:S(2)}, u32[]{:S(2)}) %collective-permute-start.17) | collective-permute-done | bytes 131104 | tf_op jit(solution)/shard_map/ppermute | solution.py:552
  96.5 5.7 %collective-permute-done.15.refs_7_ = bf16[64,1024]{1,0:T(8,128)(2,1)S(1)} collective-permute-done((bf16[64,1024]{1,0:T(8,128)(2,1)S(1)}, bf16[64,1024]{1,0:T(8,128)(2,1)S(1)}, u32[]{:S(2)}, u32[]{:S(2)}) %collective-permute-start.15) | collective-permute-done | bytes 131104 | tf_op jit(solution)/shard_map/ppermute | solution.py:552
  104.4 6.5 %collective-permute-done.13.refs_5_ = bf16[64,1024]{1,0:T(8,128)(2,1)S(1)} collective-permute-done((bf16[64,1024]{1,0:T(8,128)(2,1)S(1)}, bf16[64,1024]{1,0:T(8,128)(2,1)S(1)}, u32[]{:S(2)}, u32[]{:S(2)}) %collective-permute-start.13) | collective-permute-done | bytes 131104 | tf_op jit(solution)/shard_map/ppermute | solution.py:552
  112.9 5.3 %collective-permute-done.26.refs_1_ = bf16[96,1024]{1,0:T(8,128)(2,1)S(1)} collective-permute-done((bf16[96,1024]{1,0:T(8,128)(2,1)S(1)}, bf16[96,1024]{1,0:T(8,128)(2,1)S(1)}, u32[]{:S(2)}, u32[]{:S(2)}) %collective-permute-start.26) | collective-permute-done | bytes 196640 | tf_op jit(solution)/shard_map/ppermute | solution.py:560
  124.2 7.2 %collective-permute-start.34 = (bf16[96,1024]{1,0:T(8,128)(2,1)S(1)}, bf16[96,1024]{1,0:T(8,128)(2,1)S(1)}, u32[]{:S(2)}, u32[]{:S(2)}) collective-permute-start(bf16[96,1024]{1,0:T(8,128)(2,1)S(1)} %get-tuple-element.96), channel_id=1, source_target_pairs={{0,24},{1,25},{2,26},{3,27},{4,28},{5,29},{6,30},{7,31},{8,16},{9,... | collective-permute-start | bytes 589832 | tf_op jit(solution)/shard_map/ppermute | solution.py:560
  140.6 6.5 %collective-permute-done.25.refs_0_ = bf16[96,1024]{1,0:T(8,128)(2,1)S(1)} collective-permute-done((bf16[96,1024]{1,0:T(8,128)(2,1)S(1)}, bf16[96,1024]{1,0:T(8,128)(2,1)S(1)}, u32[]{:S(2)}, u32[]{:S(2)}) %collective-permute-start.25) | collective-permute-done | bytes 196640 | tf_op jit(solution)/shard_map/ppermute | solution.py:560
  155.9 3.3 %shard_map.190.hidden_ref = bf16[192,1024]{1,0:T(8,128)(2,1)S(1)} custom-call(bf16[96,1024]{1,0:T(8,128)(2,1)S(1)} %get-tuple-element.80.refs_0_, bf16[96,1024]{1,0:T(8,128)(2,1)S(1)} %get-tuple-element.82.refs_1_, bf16[96,1024]{1,0:T(8,128)(2,1)S(1)} %collective-permute-done.19.refs_2_, bf16[96,1024]{1,0:T(8,128)(2,1)S(1)} %collective-permute-done.20.refs_3_, ...), custom_call_target="tpu_custom_call" | custom-call | flops 1610612736 | bytes 8388608 | tf_op jit(solution)/shard_map/pallas_call | solution.py:267
  165.6 6.1 %shard_map.192.hidden_ref = bf16[576,1024]{1,0:T(8,128)(2,1)S(1)} custom-call(bf16[96,1024]{1,0:T(8,128)(2,1)S(1)} %collective-permute-done.25.refs_0_, bf16[96,1024]{1,0:T(8,128)(2,1)S(1)} %collective-permute-done.26.refs_1_, bf16[96,1024]{1,0:T(8,128)(2,1)S(1)} %collective-permute-done.27.refs_2_, bf16[96,1024]{1,0:T(8,128)(2,1)S(1)} %collective-permute-done.28.refs_3_, ...), custom_call_target="tpu_custom_call" | custom-call | flops 4831838208 | bytes 8388608 | tf_op jit(solution)/shard_map/pallas_call | solution.py:267
  171.8 4.1 %shard_map.196 = (bf16[96,1024]{1,0:T(8,128)(2,1)S(1)}, bf16[96,1024]{1,0:T(8,128)(2,1)S(1)}, bf16[96,1024]{1,0:T(8,128)(2,1)S(1)}, bf16[96,1024]{1,0:T(8,128)(2...) custom-call(bf16[576,1024]{1,0:T(8,128)(2,1)S(1)} %shard_map.192.hidden_ref, ...), custom_call_target="tpu_custom_call" | custom-call | flops 1207959552 | bytes 2097152 | tf_op jit(solution)/shard_map/pallas_call | solution.py:267
  178.3 4.1 %shard_map.193 = (bf16[96,1024]{1,0:T(8,128)(2,1)S(1)}, bf16[96,1024]{1,0:T(8,128)(2,1)S(1)}, bf16[96,1024]{1,0:T(8,128)(2,1)S(1)}, bf16[96,1024]{1,0:T(8,128)(2...) custom-call(bf16[576,1024]{1,0:T(8,128)(2,1)S(1)} %shard_map.192.hidden_ref, ...), custom_call_target="tpu_custom_call" | custom-call | flops 1207959552 | bytes 2097152 | tf_op jit(solution)/shard_map/pallas_call | solution.py:267
  188.1 10.0 %collective-permute-done.50.refs_9_ = bf16[96,1024]{1,0:T(8,128)(2,1)S(1)} collective-permute-done((bf16[96,1024]{1,0:T(8,128)(2,1)S(1)}, bf16[96,1024]{1,0:T(8,128)(2,1)S(1)}, u32[]{:S(2)}, u32[]{:S(2)}) %collective-permute-start.50) | collective-permute-done | bytes 196640 | tf_op jit(solution)/shard_map/ppermute | solution.py:560
  204.0 10.3 %collective-permute-done.39.refs_8_ = bf16[96,1024]{1,0:T(8,128)(2,1)S(1)} collective-permute-done((bf16[96,1024]{1,0:T(8,128)(2,1)S(1)}, bf16[96,1024]{1,0:T(8,128)(2,1)S(1)}, u32[]{:S(2)}, u32[]{:S(2)}) %collective-permute-start.39) | collective-permute-done | bytes 196640 | tf_op jit(solution)/shard_map/ppermute | solution.py:560
  220.8 3.3 %collective-permute-start.45 = (bf16[64,1024]{1,0:T(8,128)(2,1)S(1)}, bf16[64,1024]{1,0:T(8,128)(2,1)S(1)}, u32[]{:S(2)}, u32[]{:S(2)}) collective-permute-start(bf16[64,1024]{1,0:T(8,128)(2,1)S(1)} %get-tuple-element.108), channel_id=1, source_target_pairs={{0,6},{1,7},{2,0},{3,1},{4,2},{5,3},{6,4},{7,5},{8,14},{9,15},{10,... | collective-permute-start | bytes 393224 | tf_op jit(solution)/shard_map/ppermute | solution.py:552
  224.0 4.5 %collective-permute-done.43.refs_1_ = bf16[64,1024]{1,0:T(8,128)(2,1)S(1)} collective-permute-done((bf16[64,1024]{1,0:T(8,128)(2,1)S(1)}, bf16[64,1024]{1,0:T(8,128)(2,1)S(1)}, u32[]{:S(2)}, u32[]{:S(2)}) %collective-permute-start.43) | collective-permute-done | bytes 131104 | tf_op jit(solution)/shard_map/ppermute | solution.py:552
  228.5 4.9 %collective-permute-done.44.refs_2_ = bf16[64,1024]{1,0:T(8,128)(2,1)S(1)} collective-permute-done((bf16[64,1024]{1,0:T(8,128)(2,1)S(1)}, bf16[64,1024]{1,0:T(8,128)(2,1)S(1)}, u32[]{:S(2)}, u32[]{:S(2)}) %collective-permute-start.44) | collective-permute-done | bytes 131104 | tf_op jit(solution)/shard_map/ppermute | solution.py:552
  (154 shorter events, 94.9 us)
Async XLA Ops:
  0.0 147.1 %collective-permute-start.21 = (bf16[2,2048,512]{2,1,0:T(8,128)(2,1)}, bf16[2,2048,512]{2,1,0:T(8,128)(2,1)}, u32[]{:S(2)}, u32[]{:S(2)}) collective-permute-start(bf16[2,2048,512]{2,1,0:T(8,128)(2,1)} %refs_12_.1), channel_id=1, source_target_pairs={{0,1},{1,0},{2,3},{3,2},{4,5},{5,4},{6,7},{7,6},{8,9},{9,8},{10,11... | collective-permute-start | bytes 12582920 | tf_op jit(solution)/shard_map/ppermute | solution.py:548
  0.5 146.6 %collective-permute-start.22 = (bf16[2,2048,512]{2,1,0:T(8,128)(2,1)}, bf16[2,2048,512]{2,1,0:T(8,128)(2,1)}, u32[]{:S(2)}, u32[]{:S(2)}) collective-permute-start(bf16[2,2048,512]{2,1,0:T(8,128)(2,1)} %refs_13_.1), channel_id=1, source_target_pairs={{0,1},{1,0},{2,3},{3,2},{4,5},{5,4},{6,7},{7,6},{8,9},{9,8},{10,11... | collective-permute-start | bytes 12582920 | tf_op jit(solution)/shard_map/ppermute | solution.py:548
  0.6 149.1 %collective-permute-start.23 = (bf16[2,512,2048]{2,1,0:T(8,128)(2,1)}, bf16[2,512,2048]{2,1,0:T(8,128)(2,1)}, u32[]{:S(2)}, u32[]{:S(2)}) collective-permute-start(bf16[2,512,2048]{2,1,0:T(8,128)(2,1)} %own_ref.7), channel_id=1, source_target_pairs={{0,1},{1,0},{2,3},{3,2},{4,5},{5,4},{6,7},{7,6},{8,9},{9,8},{10,11... | collective-permute-start | bytes 12582920 | tf_op jit(solution)/shard_map/ppermute | solution.py:548
  1.0 44.2 %collective-permute-start.6 = (bf16[512,2048]{1,0:T(8,128)(2,1)}, bf16[512,2048]{1,0:T(8,128)(2,1)S(1)}, u32[]{:S(2)}, u32[]{:S(2)}) collective-permute-start(bf16[512,2048]{1,0:T(8,128)(2,1)} %own_w_ref.1), channel_id=1, source_target_pairs={{0,1},{1,0},{2,3},{3,2},{4,5},{5,4},{6,7},{7,6},{8,9},{9,8},{10,11... | collective-permute-start | bytes 6291464 | tf_op jit(solution)/shard_map/ppermute | solution.py:548
  48.1 20.0 %collective-permute-start.8 = (bf16[64,2048]{1,0:T(8,128)(2,1)S(1)}, bf16[64,2048]{1,0:T(8,128)(2,1)S(1)}, u32[]{:S(2)}, u32[]{:S(2)}) collective-permute-start(bf16[64,2048]{1,0:T(8,128)(2,1)S(1)} %get-tuple-element.76), channel_id=1, source_target_pairs={{0,4},{1,5},{2,6},{3,7},{4,0},{5,1},{6,2},{7,3},{8,12},{9,13},{10,... | collective-permute-start | bytes 786440 | tf_op jit(solution)/shard_map/ppermute | solution.py:552
  57.6 17.6 %collective-permute-start.9 = (bf16[64,2048]{1,0:T(8,128)(2,1)S(1)}, bf16[64,2048]{1,0:T(8,128)(2,1)S(1)}, u32[]{:S(2)}, u32[]{:S(2)}) collective-permute-start(bf16[64,2048]{1,0:T(8,128)(2,1)S(1)} %get-tuple-element.77), channel_id=1, source_target_pairs={{0,6},{1,7},{2,0},{3,1},{4,2},{5,3},{6,4},{7,5},{8,14},{9,15},{10,... | collective-permute-start | bytes 786440 | tf_op jit(solution)/shard_map/ppermute | solution.py:552
  139.8 24.8 %collective-permute-start.27 = (bf16[96,1024]{1,0:T(8,128)(2,1)S(1)}, bf16[96,1024]{1,0:T(8,128)(2,1)S(1)}, u32[]{:S(2)}, u32[]{:S(2)}) collective-permute-start(bf16[96,1024]{1,0:T(8,128)(2,1)S(1)} %get-tuple-element.89), channel_id=1, source_target_pairs={{0,9},{1,8},{2,11},{3,10},{4,13},{5,12},{6,15},{7,14},{8,1},{9,0},... | collective-permute-start | bytes 589832 | tf_op jit(solution)/shard_map/ppermute | solution.py:560
  147.1 17.5 %collective-permute-start.29 = (bf16[96,1024]{1,0:T(8,128)(2,1)S(1)}, bf16[96,1024]{1,0:T(8,128)(2,1)S(1)}, u32[]{:S(2)}, u32[]{:S(2)}) collective-permute-start(bf16[96,1024]{1,0:T(8,128)(2,1)S(1)} %get-tuple-element.91), channel_id=1, source_target_pairs={{0,16},{1,17},{2,18},{3,19},{4,20},{5,21},{6,22},{7,23},{8,24},{9,... | collective-permute-start | bytes 589832 | tf_op jit(solution)/shard_map/ppermute | solution.py:560
  147.1 18.0 %collective-permute-start.31 = (bf16[96,1024]{1,0:T(8,128)(2,1)S(1)}, bf16[96,1024]{1,0:T(8,128)(2,1)S(1)}, u32[]{:S(2)}, u32[]{:S(2)}) collective-permute-start(bf16[96,1024]{1,0:T(8,128)(2,1)S(1)} %get-tuple-element.93), channel_id=1, source_target_pairs={{0,17},{1,16},{2,19},{3,18},{4,21},{5,20},{6,23},{7,22},{8,25},{9,... | collective-permute-start | bytes 589832 | tf_op jit(solution)/shard_map/ppermute | solution.py:560
  147.1 18.0 %collective-permute-start.33 = (bf16[96,1024]{1,0:T(8,128)(2,1)S(1)}, bf16[96,1024]{1,0:T(8,128)(2,1)S(1)}, u32[]{:S(2)}, u32[]{:S(2)}) collective-permute-start(bf16[96,1024]{1,0:T(8,128)(2,1)S(1)} %get-tuple-element.95), channel_id=1, source_target_pairs={{0,24},{1,25},{2,26},{3,27},{4,28},{5,29},{6,30},{7,31},{8,16},{9,... | collective-permute-start | bytes 589832 | tf_op jit(solution)/shard_map/ppermute | solution.py:560
  149.7 15.4 %collective-permute-start.35 = (bf16[96,1024]{1,0:T(8,128)(2,1)S(1)}, bf16[96,1024]{1,0:T(8,128)(2,1)S(1)}, u32[]{:S(2)}, u32[]{:S(2)}) collective-permute-start(bf16[96,1024]{1,0:T(8,128)(2,1)S(1)} %get-tuple-element.97), channel_id=1, source_target_pairs={{0,25},{1,24},{2,27},{3,26},{4,29},{5,28},{6,31},{7,30},{8,17},{9,... | collective-permute-start | bytes 589832 | tf_op jit(solution)/shard_map/ppermute | solution.py:560
  164.5 17.9 %collective-permute-start.24 = (bf16[96,1024]{1,0:T(8,128)(2,1)S(1)}, bf16[96,1024]{1,0:T(8,128)(2,1)S(1)}, u32[]{:S(2)}, u32[]{:S(2)}) collective-permute-start(bf16[96,1024]{1,0:T(8,128)(2,1)S(1)} %get-tuple-element.86), channel_id=1, source_target_pairs={{0,1},{1,0},{2,3},{3,2},{4,5},{5,4},{6,7},{7,6},{8,9},{9,8},{10,11... | collective-permute-start | bytes 589832 | tf_op jit(solution)/shard_map/ppermute | solution.py:560
  164.6 19.0 %collective-permute-start.46 = (bf16[96,1024]{1,0:T(8,128)(2,1)S(1)}, bf16[96,1024]{1,0:T(8,128)(2,1)S(1)}, u32[]{:S(2)}, u32[]{:S(2)}) collective-permute-start(bf16[96,1024]{1,0:T(8,128)(2,1)S(1)} %get-tuple-element.110), channel_id=1, source_target_pairs={{0,1},{1,0},{2,3},{3,2},{4,5},{5,4},{6,7},{7,6},{8,9},{9,8},{10,11... | collective-permute-start | bytes 589832 | tf_op jit(solution)/shard_map/ppermute | solution.py:560
  182.4 15.6 %collective-permute-start.50 = (bf16[96,1024]{1,0:T(8,128)(2,1)S(1)}, bf16[96,1024]{1,0:T(8,128)(2,1)S(1)}, u32[]{:S(2)}, u32[]{:S(2)}) collective-permute-start(bf16[96,1024]{1,0:T(8,128)(2,1)S(1)} %get-tuple-element.114), channel_id=1, source_target_pairs={{0,17},{1,16},{2,19},{3,18},{4,21},{5,20},{6,23},{7,22},{8,25},{9,... | collective-permute-start | bytes 589832 | tf_op jit(solution)/shard_map/ppermute | solution.py:560
  183.6 14.4 %collective-permute-start.51 = (bf16[96,1024]{1,0:T(8,128)(2,1)S(1)}, bf16[96,1024]{1,0:T(8,128)(2,1)S(1)}, u32[]{:S(2)}, u32[]{:S(2)}) collective-permute-start(bf16[96,1024]{1,0:T(8,128)(2,1)S(1)} %get-tuple-element.115), channel_id=1, source_target_pairs={{0,24},{1,25},{2,26},{3,27},{4,28},{5,29},{6,30},{7,31},{8,16},{9,... | collective-permute-start | bytes 589832 | tf_op jit(solution)/shard_map/ppermute | solution.py:560
  185.4 14.2 %collective-permute-start.52 = (bf16[96,1024]{1,0:T(8,128)(2,1)S(1)}, bf16[96,1024]{1,0:T(8,128)(2,1)S(1)}, u32[]{:S(2)}, u32[]{:S(2)}) collective-permute-start(bf16[96,1024]{1,0:T(8,128)(2,1)S(1)} %get-tuple-element.116), channel_id=1, source_target_pairs={{0,25},{1,24},{2,27},{3,26},{4,29},{5,28},{6,31},{7,30},{8,17},{9,... | collective-permute-start | bytes 589832 | tf_op jit(solution)/shard_map/ppermute | solution.py:560
  185.5 15.4 %collective-permute-start.37 = (bf16[96,1024]{1,0:T(8,128)(2,1)S(1)}, bf16[96,1024]{1,0:T(8,128)(2,1)S(1)}, u32[]{:S(2)}, u32[]{:S(2)}) collective-permute-start(bf16[96,1024]{1,0:T(8,128)(2,1)S(1)} %get-tuple-element.99), channel_id=1, source_target_pairs={{0,8},{1,9},{2,10},{3,11},{4,12},{5,13},{6,14},{7,15},{8,0},{9,1},... | collective-permute-start | bytes 589832 | tf_op jit(solution)/shard_map/ppermute | solution.py:560
  187.2 16.7 %collective-permute-start.38 = (bf16[96,1024]{1,0:T(8,128)(2,1)S(1)}, bf16[96,1024]{1,0:T(8,128)(2,1)S(1)}, u32[]{:S(2)}, u32[]{:S(2)}) collective-permute-start(bf16[96,1024]{1,0:T(8,128)(2,1)S(1)} %get-tuple-element.100), channel_id=1, source_target_pairs={{0,9},{1,8},{2,11},{3,10},{4,13},{5,12},{6,15},{7,14},{8,1},{9,0},... | collective-permute-start | bytes 589832 | tf_op jit(solution)/shard_map/ppermute | solution.py:560
  198.0 16.2 %collective-permute-start.39 = (bf16[96,1024]{1,0:T(8,128)(2,1)S(1)}, bf16[96,1024]{1,0:T(8,128)(2,1)S(1)}, u32[]{:S(2)}, u32[]{:S(2)}) collective-permute-start(bf16[96,1024]{1,0:T(8,128)(2,1)S(1)} %get-tuple-element.101), channel_id=1, source_target_pairs={{0,16},{1,17},{2,18},{3,19},{4,20},{5,21},{6,22},{7,23},{8,24},{9,... | collective-permute-start | bytes 589832 | tf_op jit(solution)/shard_map/ppermute | solution.py:560
  198.1 18.9 %collective-permute-start.40 = (bf16[96,1024]{1,0:T(8,128)(2,1)S(1)}, bf16[96,1024]{1,0:T(8,128)(2,1)S(1)}, u32[]{:S(2)}, u32[]{:S(2)}) collective-permute-start(bf16[96,1024]{1,0:T(8,128)(2,1)S(1)} %get-tuple-element.102), channel_id=1, source_target_pairs={{0,17},{1,16},{2,19},{3,18},{4,21},{5,20},{6,23},{7,22},{8,25},{9,... | collective-permute-start | bytes 589832 | tf_op jit(solution)/shard_map/ppermute | solution.py:560
  199.6 19.1 %collective-permute-start.41 = (bf16[96,1024]{1,0:T(8,128)(2,1)S(1)}, bf16[96,1024]{1,0:T(8,128)(2,1)S(1)}, u32[]{:S(2)}, u32[]{:S(2)}) collective-permute-start(bf16[96,1024]{1,0:T(8,128)(2,1)S(1)} %get-tuple-element.103), channel_id=1, source_target_pairs={{0,24},{1,25},{2,26},{3,27},{4,28},{5,29},{6,30},{7,31},{8,16},{9,... | collective-permute-start | bytes 589832 | tf_op jit(solution)/shard_map/ppermute | solution.py:560
  200.9 17.8 %collective-permute-start.42 = (bf16[96,1024]{1,0:T(8,128)(2,1)S(1)}, bf16[96,1024]{1,0:T(8,128)(2,1)S(1)}, u32[]{:S(2)}, u32[]{:S(2)}) collective-permute-start(bf16[96,1024]{1,0:T(8,128)(2,1)S(1)} %get-tuple-element.104), channel_id=1, source_target_pairs={{0,25},{1,24},{2,27},{3,26},{4,29},{5,28},{6,31},{7,30},{8,17},{9,... | collective-permute-start | bytes 589832 | tf_op jit(solution)/shard_map/ppermute | solution.py:560
  203.9 16.9 %collective-permute-start.53 = (bf16[64,1024]{1,0:T(8,128)(2,1)S(1)}, bf16[64,1024]{1,0:T(8,128)(2,1)S(1)}, u32[]{:S(2)}, u32[]{:S(2)}) collective-permute-start(bf16[64,1024]{1,0:T(8,128)(2,1)S(1)} %get-tuple-element.118), channel_id=1, source_target_pairs={{0,2},{1,3},{2,4},{3,5},{4,6},{5,7},{6,0},{7,1},{8,10},{9,11},{10,... | collective-permute-start | bytes 393224 | tf_op jit(solution)/shard_map/ppermute | solution.py:552
  220.5 12.9 %collective-permute-start.44 = (bf16[64,1024]{1,0:T(8,128)(2,1)S(1)}, bf16[64,1024]{1,0:T(8,128)(2,1)S(1)}, u32[]{:S(2)}, u32[]{:S(2)}) collective-permute-start(bf16[64,1024]{1,0:T(8,128)(2,1)S(1)} %get-tuple-element.107), channel_id=1, source_target_pairs={{0,4},{1,5},{2,6},{3,7},{4,0},{5,1},{6,2},{7,3},{8,12},{9,13},{10,... | collective-permute-start | bytes 393224 | tf_op jit(solution)/shard_map/ppermute | solution.py:552
  (53 other events, 450.6 us)
where the time goes:
time: 235 us; the launch traced here: 234 us
  waiting for transfers between devices  108 us (46%)
  starting transfers between devices  73.3 us (31%)
  Pallas kernels  38.7 us (16%)
  local copies, waits for them, and re-layouts  13.9 us (6%)
    ppermute x18, waiting for transfers between devices, to_chip(): return lax.ppermute(value, 'tp', pairs)  54.4 us
    ppermute x28, waiting for transfers between devices, to_peer(): return lax.ppermute(value, ('sp', 'tp'), pairs)  42.9 us
    pallas_call x18, Pallas kernels, kernel(): pl.pallas_call(body, out_shape=outs, out_specs=vmem(len(outs)) if isinsta...  38.7 us
    ppermute x28, starting transfers between devices, to_peer(): return lax.ppermute(value, ('sp', 'tp'), pairs)  33 us
    ppermute x18, starting transfers between devices, to_chip(): return lax.ppermute(value, 'tp', pairs)  23.6 us
    unnamed x44, local copies, waits for them, and re-layouts  12.5 us
    ppermute x3, starting transfers between devices, mixer(): lax.ppermute(send, 'sp', [(i, i ^ k) for i in range(count)])  9.5 us
    ppermute x3, waiting for transfers between devices, mixer(): lax.ppermute(send, 'sp', [(i, i ^ k) for i in range(count)])  6.39 us
  transfers between devices with their start and end apart: 56, of which 25 were waited for; matrix products, arithmetic and copies ran while one was open for 1% of the time, Pallas kernels for 16%

commit v1 on v0

--- a/solution.py
+++ b/solution.py
@@ -14,6 +14,7 @@
 TOP = 2
 TILE = 128
 PAD = 8
+SPREAD = 2
 EXTRA = 16
 
 EPSILON = 1e-06
@@ -23,6 +24,12 @@
 
 CORES = 2
 CHUNKS = 2
+
+
+def chunk_widths(width):
+    last = max(width // 8 // (2 * TILE), 1) * 2 * TILE * SPREAD
+    second = (width - last) // 2 // (2 * TILE) * 2 * TILE
+    return (width - last - second, second, last)
 
 
 def chip_and_core(axis):
@@ -69,8 +76,18 @@
 
 
 def early_kernel(
-    raw_ref, speed_ref, fade_ref, rows_ref, cols_ref, totals_ref
+    raw_hbm, speed_hbm, fade_hbm, *refs,
 ):
+    count = (len(refs) - 7) // 2
+    in_refs, out_refs = refs[:count], refs[count : 2 * count]
+    rows_ref, cols_ref, totals_ref, raw_ref, speed_ref, fade_ref, sems = refs[2 * count :]
+    pairs = [(raw_hbm, raw_ref), (speed_hbm, speed_ref), (fade_hbm, fade_ref)]
+    pairs += list(zip(in_refs, out_refs))
+    copies = [pltpu.make_async_copy(a, b, sems.at[n]) for n, (a, b) in enumerate(pairs)]
+    for copy in copies:
+        copy.start()
+    for copy in copies[:3]:
+        copy.wait()
     heads, steps = raw_ref.shape[1:]
     lane = lax.broadcasted_iota(jnp.int32, (heads, steps), 1)
     eye = lax.broadcasted_iota(jnp.int32, (heads, heads), 0) == lax.broadcasted_iota(
@@ -100,6 +117,8 @@
         sums + weights + [jnp.zeros((STATE - 4 * heads, steps), F32)], axis=0
     )
     cols_ref[...] = stacked.T
+    for copy in copies[3:]:
+        copy.wait()
 
 
 def prepare_kernel(
@@ -269,7 +288,8 @@
         out_shape=outs,
         out_specs=vmem(len(outs)) if isinstance(outs, list) else vmem(1)[0],
         compiler_params=pltpu.CompilerParams(vmem_limit_bytes=grant * 1024 * 1024),
-        **{"in_specs": vmem(len(operands)), **settings},
+        **({} if "in_specs" in settings else dict(in_specs=vmem(len(operands)))),
+        **settings,
     )(*operands)
 
 
@@ -287,7 +307,7 @@
     last = jnp.concatenate([x[-rim:], b[-rim:], c[-rim:]], axis=1)
     low = lax.ppermute(last, "sp", [(i, i + 1) for i in range(count - 1)])
     high = lax.ppermute(first, "sp", [(i + 1, i) for i in range(count - 1)])
-    rows, cols, totals = early()
+    x, b, c, tx, tb, tc, rows, cols, totals = early(x, b, c, tx, tb, tc)
     heads = rows.shape[1]
     message = jax.ShapeDtypeStruct((groups, STATE + EXTRA, wide), BF16)
     xc, bc, cc, *sends = kernel(
@@ -341,21 +361,63 @@
     values = after.astype(F32)
     mean = jnp.sum(values * values, axis=1, keepdims=True) * (1.0 / values.shape[1])
     normed = (values * lax.rsqrt(mean + EPSILON) * gain_ref[...]).astype(BF16)
-    step = normed_refs[0].shape[1]
-    for n, ref in enumerate(normed_refs):
-        ref[...] = normed[:, n * step : (n + 1) * step]
-
-
-def final_kernel(after_ref, *refs, chunks):
+    at = 0
+    for ref in normed_refs:
+        ref[...] = normed[:, at : at + ref.shape[1]]
+        at += ref.shape[1]
+
+
+def final_kernel(after_ref, *refs, counts):
     *in_refs, out_ref = refs
-    each = len(in_refs) // chunks
-    for n in range(chunks):
-        step = in_refs[0].shape[1]
-        lanes = slice(n * step, (n + 1) * step)
+    at = 0
+    for count in counts:
+        part_refs, in_refs = in_refs[:count], in_refs[count:]
+        lanes = slice(at, at + part_refs[0].shape[1])
         total = after_ref[:, lanes].astype(F32)
-        for ref in in_refs[n * each : (n + 1) * each]:
+        for ref in part_refs:
             total = total + ref[...].astype(F32)
         out_ref[:, lanes] = total.astype(BF16)
+        at = lanes.stop
+
+
+def regroup_kernel(*refs, count, parts):
+    in_refs, out_refs = refs[:count], refs[count:]
+    rows = in_refs[0].shape[0] // parts
+    values = [ref[...].astype(F32) for ref in in_refs]
+    for n, ref in enumerate(out_refs):
+        span = slice(n * rows, (n + 1) * rows)
+        ref[...] = jnp.concatenate([value[span] for value in values], axis=0).astype(BF16)
+
+
+def spread_kernel(*refs, count):
+    total = refs[0][...].astype(F32)
+    for ref in refs[1:count]:
+        total = total + ref[...].astype(F32)
+    for n, ref in enumerate(refs[count:]):
+        rows = ref.shape[0]
+        ref[...] = total[n * rows : (n + 1) * rows].astype(BF16)
+
+
+def own_combine_kernel(meta_ref, *refs, room, axis, minor):
+    *in_refs, out_ref = refs
+    rows = out_ref.shape[0]
+    here = lax.axis_index(axis)
+    core = chip_and_core(minor)[1]
+    meta = meta_ref[...]
+    lane = lax.broadcasted_iota(jnp.int32, (rows, len(in_refs) * room), 1)
+    slot = lane
+    for o in range(len(in_refs)):
+        expert = (here ^ (o // CORES)) * CORES + (core ^ (o % CORES))
+        inside = (lane >= o * room) & (lane < (o + 1) * room)
+        slot = jnp.where(inside, lane + (expert - o) * room, slot)
+    slot = slot.astype(F32)
+    weight = jnp.where(meta[:, 0:1] == slot, meta[:, TOP : TOP + 1], 0.0) + jnp.where(
+        meta[:, 1:2] == slot, meta[:, TOP + 1 : TOP + 2], 0.0
+    )
+    values = jnp.concatenate([ref[...].astype(F32) for ref in in_refs], axis=0).astype(BF16)
+    out_ref[...] = jnp.dot(
+        weight.astype(BF16), values, preferred_element_type=F32
+    ).astype(BF16)
 
 
 def dispatch_kernel(*refs, chips, room, axis, minor):
@@ -363,9 +425,14 @@
     rows, width = x_refs[0].shape
     here = lax.axis_index(axis)
     core = chip_and_core(minor)[1]
-    meta = jnp.concatenate([ref[...] for ref in meta_refs], axis=0).T
-    rank = lax.broadcasted_iota(jnp.int32, (room, chips * rows), 0).astype(F32)
-    source = lax.broadcasted_iota(jnp.int32, (room, chips * rows), 1) // rows
+    lanes_used = max(chips * rows, TILE)
+    spare = lanes_used - chips * rows
+    metas = [ref[...] for ref in meta_refs]
+    if spare:
+        metas.append(jnp.zeros((spare, TILE), F32))
+    meta = jnp.concatenate(metas, axis=0).T
+    rank = lax.broadcasted_iota(jnp.int32, (room, lanes_used), 0).astype(F32)
+    source = lax.broadcasted_iota(jnp.int32, (room, lanes_used), 1) // rows
     chosen = []
     for o in range(len(out_refs)):
         expert = (here ^ (o // CORES)) * CORES + (core ^ (o % CORES))
@@ -377,10 +444,13 @@
     chosen = jnp.concatenate(chosen, axis=0).astype(BF16)
     for n in range(0, width, 2 * TILE):
         lanes = slice(n, n + 2 * TILE)
-        tokens = jnp.concatenate([ref[:, lanes] for ref in x_refs], axis=0)
-        out = jnp.dot(chosen, tokens, preferred_element_type=F32).astype(BF16)
+        tokens = [ref[:, lanes] for ref in x_refs]
+        if spare:
+            tokens.append(jnp.zeros((spare, 2 * TILE), BF16))
+        tokens = jnp.concatenate(tokens, axis=0)
+        out = jnp.dot(chosen, tokens, preferred_element_type=F32)
         for o, ref in enumerate(out_refs):
-            ref[:, lanes] = out[o * chips * room : (o + 1) * chips * room]
+            ref[:, lanes] = out[o * chips * room : (o + 1) * chips * room].astype(BF16)
 
 
 def combine_kernel(*refs, chips, room, axis, minor):
@@ -412,106 +482,97 @@
             ref[:, lanes] = total[r * rows : (r + 1) * rows].astype(BF16)
 
 
-def hidden_kernel(*refs, count, chunks, minor):
-    x_refs, weight_refs, refs = refs[:count], refs[count : count + 4], refs[count + 4 :]
-    hidden_ref, x_vmem, gate_vmem, up_vmem, sems = refs
+def weights_kernel(*refs, minor):
+    in_refs, (gate_ref, up_ref, down_ref, sems) = refs[:6], refs[6:]
     core = chip_and_core(minor)[1]
-    slabs, _, step = gate_vmem.shape
+    slabs, _, step = gate_ref.shape
     per_source = slabs // 2
+    half = down_ref.shape[0] // 2
     copies = []
-    for t in range(slabs):
-        gate, up = weight_refs[0:2] if t < per_source else weight_refs[2:4]
-        span = pl.ds((t % per_source) * step, step)
-        copies.append(
-            [
-                pltpu.make_async_copy(gate.at[core, :, span], gate_vmem.at[t], sems.at[t, 0]),
-                pltpu.make_async_copy(up.at[core, :, span], up_vmem.at[t], sems.at[t, 1]),
-            ]
-        )
-    for group in copies:
-        for copy in group:
-            copy.start()
-    rows, columns = x_refs[0].shape
-    for o, ref in enumerate(x_refs):
-        at, n = o // chunks * rows, o % chunks * columns
-        x_vmem[at : at + rows, n : n + columns] = ref[...]
-    for t in range(slabs):
-        for copy in copies[t]:
-            copy.wait()
-        gate = jnp.dot(x_vmem[...], gate_vmem[t], preferred_element_type=F32)
-        up = jnp.dot(x_vmem[...], up_vmem[t], preferred_element_type=F32)
-        hidden_ref[:, t * step : (t + 1) * step] = (silu(gate) * up).astype(BF16)
-
-
-def down_kernel(hidden_ref, own_ref, other_ref, *refs, chunk, minor):
-    *out_refs, down_vmem, sems = refs
-    core = chip_and_core(minor)[1]
-    rows, columns = out_refs[0].shape
-    half, step = down_vmem.shape[0] // 2, 2 * TILE
-    copies = []
-    for n in range(0, columns, step):
-        for side, ref in enumerate((own_ref, other_ref)):
-            copies.append(
-                pltpu.make_async_copy(
-                    ref.at[core, :, pl.ds(chunk * columns + n, step)],
-                    down_vmem.at[pl.ds(side * half, half), pl.ds(n, step)],
-                    sems.at[n // step, side],
-                )
-            )
+    for side in range(2):
+        gate, up, down = in_refs[3 * side : 3 * side + 3]
+        for t in range(per_source):
+            at, span = side * per_source + t, pl.ds(t * step, step)
+            copies.append((gate.at[core, :, span], gate_ref.at[at]))
+            copies.append((up.at[core, :, span], up_ref.at[at]))
+        copies.append((down.at[core], down_ref.at[pl.ds(side * half, half)]))
+    copies = [pltpu.make_async_copy(a, b, sems.at[n]) for n, (a, b) in enumerate(copies)]
     for copy in copies:
         copy.start()
-    for n in range(0, columns, step):
-        copies[n // step * 2].wait()
-        copies[n // step * 2 + 1].wait()
+    for copy in copies:
+        copy.wait()
+
+
+def hidden_kernel(*refs, count, chunks):
+    x_refs, (gate_ref, up_ref, hidden_ref, x_vmem) = refs[:count], refs[count:]
+    slabs, _, step = gate_ref.shape
+    rows, at = x_refs[0].shape[0], 0
+    for n in range(chunks):
+        columns = x_refs[n].shape[1]
+        for o, ref in enumerate(x_refs[n::chunks]):
+            x_vmem[o * rows : (o + 1) * rows, at : at + columns] = ref[...]
+        at += columns
+    for t in range(slabs):
+        gate = jnp.dot(x_vmem[...], gate_ref[t], preferred_element_type=F32)
+        up = jnp.dot(x_vmem[...], up_ref[t], preferred_element_type=F32)
+        hidden_ref[:, t * step : (t + 1) * step] = (silu(gate) * up).astype(BF16)
+
+
+def down_kernel(hidden_ref, down_ref, *out_refs, first):
+    rows, columns = out_refs[0].shape
+    for n in range(0, columns, 2 * TILE):
+        at = first + n
         part = jnp.dot(
-            hidden_ref[...], down_vmem[:, n : n + step], preferred_element_type=F32
+            hidden_ref[...], down_ref[:, at : at + 2 * TILE], preferred_element_type=F32
         ).astype(BF16)
         for o, ref in enumerate(out_refs):
-            ref[:, n : n + step] = part[o * rows : (o + 1) * rows]
-
-
-def run_experts(messages, own, other, chunks):
-    flat = [part for message in messages for part in message]
-    rows, columns = flat[0].shape
-    total_rows, width = len(messages) * rows, columns * chunks
-    hidden = own[0].shape[2]
+            ref[:, n : n + 2 * TILE] = part[o * rows : (o + 1) * rows]
+
+
+def side_by_side(own, other):
+    _, width, hidden = own[0].shape
     step = 2 * TILE if hidden % (2 * TILE) == 0 else hidden
     slabs = 2 * (hidden // step)
+    return kernel(
+        functools.partial(weights_kernel, minor="tp"),
+        (*own, *other),
+        [jax.ShapeDtypeStruct((slabs, width, step), BF16)] * 2
+        + [jax.ShapeDtypeStruct((2 * hidden, width), BF16)],
+        grant=28,
+        in_specs=[pl.BlockSpec(memory_space=pltpu.HBM)] * 6,
+        scratch_shapes=[pltpu.SemaphoreType.DMA((2 * slabs + 2,))],
+    )
+
+
+def run_experts(messages, gate, up, down):
+    flat = [part for message in messages for part in message]
+    widths = [part.shape[1] for part in messages[0]]
+    rows, width = flat[0].shape[0], sum(widths)
+    total_rows, hidden = len(messages) * rows, down.shape[0]
     inner = kernel(
-        functools.partial(hidden_kernel, count=len(flat), chunks=chunks, minor="tp"),
-        (*flat, own[0], own[1], other[0], other[1]),
-        jax.ShapeDtypeStruct((total_rows, 2 * hidden), BF16),
-        grant=28,
-        in_specs=vmem(len(flat)) + [pl.BlockSpec(memory_space=pltpu.HBM)] * 4,
-        scratch_shapes=[
-            pltpu.VMEM((total_rows, width), BF16),
-            pltpu.VMEM((slabs, width, step), BF16),
-            pltpu.VMEM((slabs, width, step), BF16),
-            pltpu.SemaphoreType.DMA((slabs, 2)),
-        ],
+        functools.partial(hidden_kernel, count=len(flat), chunks=len(widths)),
+        (*flat, gate, up),
+        jax.ShapeDtypeStruct((total_rows, hidden), BF16),
+        grant=24,
+        scratch_shapes=[pltpu.VMEM((total_rows, width), BF16)],
         cost_estimate=pl.CostEstimate(
-            flops=8 * total_rows * width * hidden,
-            bytes_accessed=8 * hidden * width,
-            transcendentals=total_rows * 2 * hidden,
+            flops=4 * total_rows * width * hidden,
+            bytes_accessed=4 * hidden * width,
+            transcendentals=total_rows * hidden,
         ),
     )
     return [
         kernel(
-            functools.partial(down_kernel, chunk=n, minor="tp"),
-            (inner, own[2], other[2]),
+            functools.partial(down_kernel, first=sum(widths[:n])),
+            (inner, down),
             [jax.ShapeDtypeStruct((rows, columns), BF16)] * len(messages),
-            in_specs=vmem(1) + [pl.BlockSpec(memory_space=pltpu.HBM)] * 2,
-            scratch_shapes=[
-                pltpu.VMEM((2 * hidden, columns), BF16),
-                pltpu.SemaphoreType.DMA((columns // (2 * TILE), 2)),
-            ],
             cost_estimate=pl.CostEstimate(
-                flops=4 * total_rows * columns * hidden,
-                bytes_accessed=4 * hidden * columns,
+                flops=2 * total_rows * columns * hidden,
+                bytes_accessed=2 * hidden * columns,
                 transcendentals=0,
             ),
         )
-        for n in range(chunks)
+        for n, columns in enumerate(widths)
     ]
 
 
@@ -560,18 +621,23 @@
         return lax.ppermute(value, ("sp", "tp"), pairs)
 
     piece = jax.ShapeDtypeStruct((rows, width), BF16)
-    slim = jax.ShapeDtypeStruct((rows, width // CHUNKS), BF16)
-    message = jax.ShapeDtypeStruct((chips * room, width // CHUNKS), BF16)
-
-    def early():
+    widths = chunk_widths(width)
+    slim = [jax.ShapeDtypeStruct((rows, columns), BF16) for columns in widths]
+
+    def early(*inputs):
+        small = (raw_increments, channel_log_fade_speed, extra_log_fade)
         return kernel(
             early_kernel,
-            (raw_increments, channel_log_fade_speed, extra_log_fade),
-            [
+            (*small, *inputs),
+            [jax.ShapeDtypeStruct(v.shape, v.dtype) for v in inputs]
+            + [
                 jax.ShapeDtypeStruct(raw_increments.shape, F32),
                 jax.ShapeDtypeStruct((raw_increments.shape[2], STATE), F32),
                 jax.ShapeDtypeStruct((*raw_increments.shape[:2], STATE), F32),
             ],
+            in_specs=[pl.BlockSpec(memory_space=pltpu.HBM)] * (len(small) + len(inputs)),
+            scratch_shapes=[pltpu.VMEM(v.shape, v.dtype) for v in small]
+            + [pltpu.SemaphoreType.DMA((len(small) + len(inputs),))],
         )
 
     keep, send = mixer(
@@ -597,7 +663,7 @@
     after, *normed = kernel(
         functools.partial(after_kernel, chips=chips),
         (skip_stream_entry, routing_scaling_factor.reshape(1, -1), *parts),
-        [piece] + [slim] * CHUNKS,
+        [piece] + slim,
     )
     meta = kernel(
         functools.partial(route_kernel, room=room),
@@ -606,30 +672,65 @@
     )
     metas = [meta] + [to_chip(meta, r) for r in range(1, chips)]
     places = dict(chips=chips, room=room, axis="sp", minor="tp")
+    few = jax.ShapeDtypeStruct((room, widths[-1]), BF16)
+    stack = jax.ShapeDtypeStruct((experts * room, widths[-1]), BF16)
+    message = jax.ShapeDtypeStruct((chips * room, widths[-1]), BF16)
+    sends = kernel(
+        functools.partial(dispatch_kernel, **{**places, "chips": 1}),
+        (meta, normed[-1]),
+        [few] * experts,
+    )
+    sends = [sends[0]] + [to_peer(sends[o], o) for o in range(1, experts)]
+    (stacked,) = kernel(functools.partial(regroup_kernel, count=experts, parts=1), sends, [stack])
+    stacked = [stacked] + [to_chip(stacked, r) for r in range(1, chips)]
+    last = kernel(
+        functools.partial(regroup_kernel, count=chips, parts=experts), stacked, [message] * experts
+    )
+
     messages = []
     for n in range(CHUNKS):
+        message = jax.ShapeDtypeStruct((chips * room, widths[n]), BF16)
         tokens = [normed[n]] + [to_chip(normed[n], r) for r in range(1, chips)]
         sends = kernel(
             functools.partial(dispatch_kernel, **places), (*metas, *tokens), [message] * experts
         )
         messages.append([sends[0]] + [to_peer(sends[o], o) for o in range(1, experts)])
+    messages.append(last)
+    gate, up, down = side_by_side(own, other)
     bounds = group_bounds(peers)
-    results = [[] for _ in range(CHUNKS)]
-    for first, last in zip(bounds[:-1], bounds[1:]):
-        part = [[messages[n][o] for n in range(CHUNKS)] for o in range(first, last)]
-        done = run_experts(part, own, other, CHUNKS)
-        for n in range(CHUNKS):
-            results[n] += done[n]
+    results = [[] for _ in widths]
+    for first, end in zip(bounds[:-1], bounds[1:]):
+        part = [[chunk[o] for chunk in messages] for o in range(first, end)]
+        done = run_experts(part, gate, up, down)
+        for chunk, more in zip(results, done):
+            chunk += more
+    shares = kernel(
+        functools.partial(regroup_kernel, count=experts, parts=chips), results[-1], [stack] * chips
+    )
+    shares = [shares[0]] + [to_chip(shares[chips - r], r) for r in range(1, chips)]
+    sends = kernel(functools.partial(spread_kernel, count=chips), shares, [few] * experts)
+    back = [sends[0]] + [to_peer(sends[o], o) for o in range(1, experts)]
+    last = kernel(
+        functools.partial(own_combine_kernel, room=room, axis="sp", minor="tp"),
+        (meta, *back),
+        slim[-1],
+    )
     pieces = []
     for n in range(CHUNKS):
         back = [results[n][0]] + [to_peer(results[n][o], o) for o in range(1, experts)]
-        sums = kernel(functools.partial(combine_kernel, **places), (*metas, *back), [slim] * chips)
+        sums = kernel(
+            functools.partial(combine_kernel, **places), (*metas, *back), [slim[n]] * chips
+        )
         pieces += [sums[0]] + [to_chip(sums[chips - r], r) for r in range(1, chips)]
-    return kernel(functools.partial(final_kernel, chunks=CHUNKS), (after, *pieces), piece)
+    return kernel(
+        functools.partial(final_kernel, counts=(chips,) * CHUNKS + (1,)),
+        (after, *pieces, last),
+        piece,
+    )
 
 
 def group_bounds(peers):
-    return [0, CORES, CORES * peers]
+    return [0, CORES, CORES * (peers // 2 + 1), CORES * peers]
 
 
 def solution(mesh):

time: 235 us -> 237 us (level)
  starting transfers between devices: 73.3 us -> 95.2 us
  waiting for transfers between devices: 108 us -> 93.6 us
  Pallas kernels: 38.7 us -> 31.5 us
    ppermute x18 -> x24, starting transfers between devices: 23.6 us -> 39 us  [to_chip(): return lax.ppermute(value, 'tp', pairs)]
    ppermute x28 -> x42, waiting for transfers between devices: 42.9 us -> 27.7 us  [to_peer(): return lax.ppermute(value, ('sp', 'tp'), pairs)]
    pallas_call x18 -> x31, Pallas kernels: 38.7 us -> 31.5 us  [kernel(): pl.pallas_call(body, out_shape=outs, out_specs=vmem(len(outs)) if isinsta...]
    ppermute x28 -> x42, starting transfers between devices: 33 us -> 38 us  [to_peer(): return lax.ppermute(value, ('sp', 'tp'), pairs)]
    ppermute x18 -> x24, waiting for transfers between devices: 54.4 us -> 56.8 us  [to_chip(): return lax.ppermute(value, 'tp', pairs)]
    unnamed x44 -> x40, local copies, waits for them, and re-layouts: 12.5 us -> 13.9 us
  transfers between devices with their start and end apart: 56 -> 76, of which waited for: 25 -> 32; matrix products, arithmetic and copies ran while one was open for 1% -> 1% of each run, Pallas kernels for 16% -> 13%
where the time goes in v1:
time: 237 us; the launch traced here: 236 us
  starting transfers between devices  95.2 us (40%)
  waiting for transfers between devices  93.6 us (39%)
  Pallas kernels  31.5 us (13%)
  local copies, waits for them, and re-layouts  15.4 us (6%)
    ppermute x24, waiting for transfers between devices, to_chip(): return lax.ppermute(value, 'tp', pairs)  56.8 us
    ppermute x24, starting transfers between devices, to_chip(): return lax.ppermute(value, 'tp', pairs)  39 us
    ppermute x42, starting transfers between devices, to_peer(): return lax.ppermute(value, ('sp', 'tp'), pairs)  38 us
    pallas_call x31, Pallas kernels, kernel(): pl.pallas_call(body, out_shape=outs, out_specs=vmem(len(outs)) if isinsta...  31.5 us
    ppermute x42, waiting for transfers between devices, to_peer(): return lax.ppermute(value, ('sp', 'tp'), pairs)  27.7 us
    unnamed x40, local copies, waits for them, and re-layouts  13.9 us
    ppermute x3, starting transfers between devices, mixer(): lax.ppermute(send, 'sp', [(i, i ^ k) for i in range(count)])  11 us
    ppermute x3, waiting for transfers between devices, mixer(): lax.ppermute(send, 'sp', [(i, i ^ k) for i in range(count)])  6.25 us
  transfers between devices with their start and end apart: 76, of which 32 were waited for; matrix products, arithmetic and copies ran while one was open for 1% of the time, Pallas kernels for 13%

profile of v1, /device:TPU:0, one launch (start us, length us, event | category | flops | bytes accessed | tf_op | source)
XLA Modules:
  0.0 236.3 jit_solution(14696605006786969237)
XLA Ops:
  2.5 4.9 %collective-permute-start = (bf16[2,1024]{1,0:T(2,128)(2,1)S(1)}, bf16[2,1024]{1,0:T(2,128)(2,1)S(1)}, u32[]{:S(2)}, u32[]{:S(2)}) collective-permute-start(bf16[2,1024]{1,0:T(2,128)(2,1)S(1)} %pad_maximum_fusion), channel_id=1, source_target_pairs={{0,8},{8,16},{16,24},{1,9},{9,17},{17,25},{2,10},{10,18},{18,26},{... | collective-permute-start | bytes 12296 | tf_op jit(solution)/shard_map/ppermute | solution.py:308
  18.2 3.1 %shard_map.182 = (bf16[512,512]{1,0:T(8,128)(2,1)S(1)}, bf16[512,256]{1,0:T(8,128)(2,1)S(1)}, bf16[512,256]{1,0:T(8,128)(2,1)S(1)}, bf16[2,144,256]{2,1,0:T(8,12...) custom-call(bf16[512,512]{1,0:T(8,128)(2,1)S(1)} %get-tuple-element.109.x_ref, ...), custom_call_target="tpu_custom_call" | custom-call | tf_op jit(solution)/shard_map/pallas_call | solution.py:286
  21.3 3.0 %collective-permute-start.2 = (bf16[2,144,256]{2,1,0:T(8,128)(2,1)S(1)}, bf16[2,144,256]{2,1,0:T(8,128)(2,1)S(1)}, u32[]{:S(2)}, u32[]{:S(2)}) collective-permute-start(bf16[2,144,256]{2,1,0:T(8,128)(2,1)S(1)} %get-tuple-element.121), channel_id=1, source_target_pairs={{0,8},{8,0},{16,24},{24,16},{1,9},{9,1},{17,25},{25,17},{2,10},{10... | collective-permute-start | bytes 442376 | tf_op jit(solution)/shard_map/ppermute | solution.py:320
  24.3 3.1 %collective-permute-done.2.rest_0_ = bf16[2,144,256]{2,1,0:T(8,128)(2,1)S(1)} collective-permute-done((bf16[2,144,256]{2,1,0:T(8,128)(2,1)S(1)}, bf16[2,144,256]{2,1,0:T(8,128)(2,1)S(1)}, u32[]{:S(2)}, u32[]{:S(2)}) %collective-permute-start.2) | collective-permute-done | bytes 147488 | tf_op jit(solution)/shard_map/ppermute | solution.py:320
  27.4 3.5 %collective-permute-start.3 = (bf16[2,144,256]{2,1,0:T(8,128)(2,1)S(1)}, bf16[2,144,256]{2,1,0:T(8,128)(2,1)S(1)}, u32[]{:S(2)}, u32[]{:S(2)}) collective-permute-start(bf16[2,144,256]{2,1,0:T(8,128)(2,1)S(1)} %get-tuple-element.122), channel_id=1, source_target_pairs={{0,16},{8,24},{16,0},{24,8},{1,17},{9,25},{17,1},{25,9},{2,18},{10... | collective-permute-start | bytes 442376 | tf_op jit(solution)/shard_map/ppermute | solution.py:320
  30.9 3.1 %collective-permute-done.3.rest_1_ = bf16[2,144,256]{2,1,0:T(8,128)(2,1)S(1)} collective-permute-done((bf16[2,144,256]{2,1,0:T(8,128)(2,1)S(1)}, bf16[2,144,256]{2,1,0:T(8,128)(2,1)S(1)}, u32[]{:S(2)}, u32[]{:S(2)}) %collective-permute-start.3) | collective-permute-done | bytes 147488 | tf_op jit(solution)/shard_map/ppermute | solution.py:320
  34.0 4.5 %collective-permute-start.4 = (bf16[2,144,256]{2,1,0:T(8,128)(2,1)S(1)}, bf16[2,144,256]{2,1,0:T(8,128)(2,1)S(1)}, u32[]{:S(2)}, u32[]{:S(2)}) collective-permute-start(bf16[2,144,256]{2,1,0:T(8,128)(2,1)S(1)} %get-tuple-element.123), channel_id=1, source_target_pairs={{0,24},{8,16},{16,8},{24,0},{1,25},{9,17},{17,9},{25,1},{2,26},{10... | collective-permute-start | bytes 442376 | tf_op jit(solution)/shard_map/ppermute | solution.py:320
  38.6 3.1 %shard_map.183.y_ref = f32[512,512]{1,0:T(8,128)S(1)} custom-call(bf16[512,512]{1,0:T(8,128)(2,1)S(1)} %get-tuple-element.117.xc_ref, bf16[512,256]{1,0:T(8,128)(2,1)S(1)} %get-tuple-element.118.bc_ref, bf16[512,256]{1,0:T(8,128)(2,1)S(1)} %get-tuple-element.119.cc_ref, f32[2,8,512]{2,1,0:T(8,128)S(1)} %get-tuple-element.120.rows_ref, ...), custom_call_target="tpu_custom_call" | custom-call | flops 1610612736 | bytes 2097152 | tf_op jit(solution)/shard_map/pallas_call | solution.py:286
  51.2 6.5 %collective-permute-done.12.refs_3_ = f32[64,128]{1,0:T(8,128)S(1)} collective-permute-done((f32[64,128]{1,0:T(8,128)S(1)}, f32[64,128]{1,0:T(8,128)S(1)}, u32[]{:S(2)}, u32[]{:S(2)}) %collective-permute-start.12) | collective-permute-done | bytes 32800 | tf_op jit(solution)/shard_map/ppermute | solution.py:613
  60.6 11.9 %collective-permute-done.8.refs_2_ = bf16[64,2048]{1,0:T(8,128)(2,1)S(1)} collective-permute-done((bf16[64,2048]{1,0:T(8,128)(2,1)S(1)}, bf16[64,2048]{1,0:T(8,128)(2,1)S(1)}, u32[]{:S(2)}, u32[]{:S(2)}) %collective-permute-start.8) | collective-permute-done | bytes 262176 | tf_op jit(solution)/shard_map/ppermute | solution.py:613
  72.5 7.3 %collective-permute-start.10 = (f32[64,128]{1,0:T(8,128)S(1)}, f32[64,128]{1,0:T(8,128)S(1)}, u32[]{:S(2)}, u32[]{:S(2)}) collective-permute-start(f32[64,128]{1,0:T(8,128)S(1)} %shard_map.187.refs_0_.meta_ref), channel_id=1, source_target_pairs={{0,2},{1,3},{2,4},{3,5},{4,6},{5,7},{6,0},{7,1},{8,10},{9,11},{10,... | collective-permute-start | bytes 98312 | tf_op jit(solution)/shard_map/ppermute | solution.py:613
  82.4 3.2 %collective-permute-done.20.refs_2_ = bf16[24,512]{1,0:T(8,128)(2,1)S(1)} collective-permute-done((bf16[24,512]{1,0:T(8,128)(2,1)S(1)}, bf16[24,512]{1,0:T(8,128)(2,1)S(1)}, u32[]{:S(2)}, u32[]{:S(2)}) %collective-permute-start.20) | collective-permute-done | bytes 24608 | tf_op jit(solution)/shard_map/ppermute | solution.py:621
  89.4 2.9 %collective-permute-start.24 = (bf16[24,512]{1,0:T(8,128)(2,1)S(1)}, bf16[24,512]{1,0:T(8,128)(2,1)S(1)}, u32[]{:S(2)}, u32[]{:S(2)}) collective-permute-start(bf16[24,512]{1,0:T(8,128)(2,1)S(1)} %get-tuple-element.142), channel_id=1, source_target_pairs={{0,24},{1,25},{2,26},{3,27},{4,28},{5,29},{6,30},{7,31},{8,16},{9,... | collective-permute-start | bytes 73736 | tf_op jit(solution)/shard_map/ppermute | solution.py:621
  100.0 3.1 %collective-permute-start.13 = (bf16[64,768]{1,0:T(8,128)(2,1)S(1)}, bf16[64,768]{1,0:T(8,128)(2,1)S(1)}, u32[]{:S(2)}, u32[]{:S(2)}) collective-permute-start(bf16[64,768]{1,0:T(8,128)(2,1)S(1)} %get-tuple-element.131.refs_4_), channel_id=1, source_target_pairs={{0,2},{1,3},{2,4},{3,5},{4,6},{5,7},{6,0},{7,1},{8,10},{9,11},{10,... | collective-permute-start | bytes 294920 | tf_op jit(solution)/shard_map/ppermute | solution.py:613
  107.2 5.0 %collective-permute-done.18.refs_7_ = bf16[64,768]{1,0:T(8,128)(2,1)S(1)} collective-permute-done((bf16[64,768]{1,0:T(8,128)(2,1)S(1)}, bf16[64,768]{1,0:T(8,128)(2,1)S(1)}, u32[]{:S(2)}, u32[]{:S(2)}) %collective-permute-start.18) | collective-permute-done | bytes 98336 | tf_op jit(solution)/shard_map/ppermute | solution.py:613
  115.5 6.6 %collective-permute-done.16.refs_5_ = bf16[64,768]{1,0:T(8,128)(2,1)S(1)} collective-permute-done((bf16[64,768]{1,0:T(8,128)(2,1)S(1)}, bf16[64,768]{1,0:T(8,128)(2,1)S(1)}, u32[]{:S(2)}, u32[]{:S(2)}) %collective-permute-start.16) | collective-permute-done | bytes 98336 | tf_op jit(solution)/shard_map/ppermute | solution.py:613
  125.7 7.1 %collective-permute-done.27.refs_2_ = bf16[192,512]{1,0:T(8,128)(2,1)S(1)} collective-permute-done((bf16[192,512]{1,0:T(8,128)(2,1)S(1)}, bf16[192,512]{1,0:T(8,128)(2,1)S(1)}, u32[]{:S(2)}, u32[]{:S(2)}) %collective-permute-start.27) | collective-permute-done | bytes 196640 | tf_op jit(solution)/shard_map/ppermute | solution.py:613
  143.7 3.4 %shard_map.193 = (bf16[4,2048,256]{2,1,0:T(8,128)(2,1)S(1)}, bf16[4,2048,256]{2,1,0:T(8,128)(2,1)S(1)}, bf16[1024,2048]{1,0:T(8,128)(2,1)S(1)}) custom-call(bf16[2,2048,512]{2,1,0:T(8,128)(2,1)S(1)} %copy-done, bf16[2,2048,512]{2,1,0:T(8,128)(2,1)S(1)} %copy-done.1, bf16[2,512,2048]{2,1,0:T(8,128)(2,1)S(1)} %copy-done.2, ...), custom_call_target="tpu_custom_call" | custom-call | tf_op jit(solution)/shard_map/pallas_call | solution.py:286
  171.2 8.0 %collective-permute-done.41.refs_9_ = bf16[96,768]{1,0:T(8,128)(2,1)S(1)} collective-permute-done((bf16[96,768]{1,0:T(8,128)(2,1)S(1)}, bf16[96,768]{1,0:T(8,128)(2,1)S(1)}, u32[]{:S(2)}, u32[]{:S(2)}) %collective-permute-start.41) | collective-permute-done | bytes 147488 | tf_op jit(solution)/shard_map/ppermute | solution.py:621
  179.9 3.4 %shard_map.196.hidden_ref = bf16[384,1024]{1,0:T(8,128)(2,1)S(1)} custom-call(bf16[96,768]{1,0:T(8,128)(2,1)S(1)} %collective-permute-done.35.refs_0_, bf16[96,768]{1,0:T(8,128)(2,1)S(1)} %collective-permute-done.36.refs_1_, bf16[96,512]{1,0:T(8,128)(2,1)S(1)} %get-tuple-element.155.refs_2_, bf16[96,768]{1,0:T(8,128)(2,1)S(1)} %collective-permute-done.37.refs_3_, ...), custom_call_target="tpu_custom_call" | custom-call | flops 3221225472 | bytes 8388608 | tf_op jit(solution)/shard_map/pallas_call | solution.py:286
  195.4 3.1 %collective-permute-done.58.refs_7_ = bf16[96,768]{1,0:T(8,128)(2,1)S(1)} collective-permute-done((bf16[96,768]{1,0:T(8,128)(2,1)S(1)}, bf16[96,768]{1,0:T(8,128)(2,1)S(1)}, u32[]{:S(2)}, u32[]{:S(2)}) %collective-permute-start.58) | collective-permute-done | bytes 147488 | tf_op jit(solution)/shard_map/ppermute | solution.py:621
  202.8 3.9 %collective-permute-done.67.refs_2_ = bf16[192,512]{1,0:T(8,128)(2,1)S(1)} collective-permute-done((bf16[192,512]{1,0:T(8,128)(2,1)S(1)}, bf16[192,512]{1,0:T(8,128)(2,1)S(1)}, u32[]{:S(2)}, u32[]{:S(2)}) %collective-permute-start.67) | collective-permute-done | bytes 196640 | tf_op jit(solution)/shard_map/ppermute | solution.py:613
  224.2 2.9 %collective-permute-start.55 = (bf16[64,768]{1,0:T(8,128)(2,1)S(1)}, bf16[64,768]{1,0:T(8,128)(2,1)S(1)}, u32[]{:S(2)}, u32[]{:S(2)}) collective-permute-start(bf16[64,768]{1,0:T(8,128)(2,1)S(1)} %get-tuple-element.180), channel_id=1, source_target_pairs={{0,6},{1,7},{2,0},{3,1},{4,2},{5,3},{6,4},{7,5},{8,14},{9,15},{10,... | collective-permute-start | bytes 294920 | tf_op jit(solution)/shard_map/ppermute | solution.py:613
  230.3 5.2 %collective-permute-done.54.refs_2_ = bf16[64,768]{1,0:T(8,128)(2,1)S(1)} collective-permute-done((bf16[64,768]{1,0:T(8,128)(2,1)S(1)}, bf16[64,768]{1,0:T(8,128)(2,1)S(1)}, u32[]{:S(2)}, u32[]{:S(2)}) %collective-permute-start.54) | collective-permute-done | bytes 98336 | tf_op jit(solution)/shard_map/ppermute | solution.py:613
  (203 shorter events, 124.1 us)
Async XLA Ops:
  0.0 134.1 %collective-permute-start.31 = (bf16[2,2048,512]{2,1,0:T(8,128)(2,1)}, bf16[2,2048,512]{2,1,0:T(8,128)(2,1)}, u32[]{:S(2)}, u32[]{:S(2)}) collective-permute-start(bf16[2,2048,512]{2,1,0:T(8,128)(2,1)} %refs_0_.3), channel_id=1, source_target_pairs={{0,1},{1,0},{2,3},{3,2},{4,5},{5,4},{6,7},{7,6},{8,9},{9,8},{10,11... | collective-permute-start | bytes 12582920 | tf_op jit(solution)/shard_map/ppermute | solution.py:609
  0.5 134.2 %collective-permute-start.32 = (bf16[2,2048,512]{2,1,0:T(8,128)(2,1)}, bf16[2,2048,512]{2,1,0:T(8,128)(2,1)}, u32[]{:S(2)}, u32[]{:S(2)}) collective-permute-start(bf16[2,2048,512]{2,1,0:T(8,128)(2,1)} %refs_1_.3), channel_id=1, source_target_pairs={{0,1},{1,0},{2,3},{3,2},{4,5},{5,4},{6,7},{7,6},{8,9},{9,8},{10,11... | collective-permute-start | bytes 12582920 | tf_op jit(solution)/shard_map/ppermute | solution.py:609
  0.5 134.6 %collective-permute-start.33 = (bf16[2,512,2048]{2,1,0:T(8,128)(2,1)}, bf16[2,512,2048]{2,1,0:T(8,128)(2,1)}, u32[]{:S(2)}, u32[]{:S(2)}) collective-permute-start(bf16[2,512,2048]{2,1,0:T(8,128)(2,1)} %refs_2_.3), channel_id=1, source_target_pairs={{0,1},{1,0},{2,3},{3,2},{4,5},{5,4},{6,7},{7,6},{8,9},{9,8},{10,11... | collective-permute-start | bytes 12582920 | tf_op jit(solution)/shard_map/ppermute | solution.py:609
  1.0 44.5 %collective-permute-start.6 = (bf16[512,2048]{1,0:T(8,128)(2,1)}, bf16[512,2048]{1,0:T(8,128)(2,1)S(1)}, u32[]{:S(2)}, u32[]{:S(2)}) collective-permute-start(bf16[512,2048]{1,0:T(8,128)(2,1)} %own_w_ref.1), channel_id=1, source_target_pairs={{0,1},{1,0},{2,3},{3,2},{4,5},{5,4},{6,7},{7,6},{8,9},{9,8},{10,11... | collective-permute-start | bytes 6291464 | tf_op jit(solution)/shard_map/ppermute | solution.py:609
  46.7 11.6 %collective-permute-start.7 = (bf16[64,2048]{1,0:T(8,128)(2,1)S(1)}, bf16[64,2048]{1,0:T(8,128)(2,1)S(1)}, u32[]{:S(2)}, u32[]{:S(2)}) collective-permute-start(bf16[64,2048]{1,0:T(8,128)(2,1)S(1)} %get-tuple-element.127), channel_id=1, source_target_pairs={{0,2},{1,3},{2,4},{3,5},{4,6},{5,7},{6,0},{7,1},{8,10},{9,11},{10,... | collective-permute-start | bytes 786440 | tf_op jit(solution)/shard_map/ppermute | solution.py:613
  57.7 14.8 %collective-permute-start.8 = (bf16[64,2048]{1,0:T(8,128)(2,1)S(1)}, bf16[64,2048]{1,0:T(8,128)(2,1)S(1)}, u32[]{:S(2)}, u32[]{:S(2)}) collective-permute-start(bf16[64,2048]{1,0:T(8,128)(2,1)S(1)} %get-tuple-element.128), channel_id=1, source_target_pairs={{0,4},{1,5},{2,6},{3,7},{4,0},{5,1},{6,2},{7,3},{8,12},{9,13},{10,... | collective-permute-start | bytes 786440 | tf_op jit(solution)/shard_map/ppermute | solution.py:613
  58.3 14.2 %collective-permute-start.9 = (bf16[64,2048]{1,0:T(8,128)(2,1)S(1)}, bf16[64,2048]{1,0:T(8,128)(2,1)S(1)}, u32[]{:S(2)}, u32[]{:S(2)}) collective-permute-start(bf16[64,2048]{1,0:T(8,128)(2,1)S(1)} %get-tuple-element.129), channel_id=1, source_target_pairs={{0,6},{1,7},{2,0},{3,1},{4,2},{5,3},{6,4},{7,5},{8,14},{9,15},{10,... | collective-permute-start | bytes 786440 | tf_op jit(solution)/shard_map/ppermute | solution.py:613
  132.9 14.2 %collective-permute-start.30 = (bf16[96,768]{1,0:T(8,128)(2,1)S(1)}, bf16[96,768]{1,0:T(8,128)(2,1)S(1)}, u32[]{:S(2)}, u32[]{:S(2)}) collective-permute-start(bf16[96,768]{1,0:T(8,128)(2,1)S(1)} %get-tuple-element.146), channel_id=1, source_target_pairs={{0,1},{1,0},{2,3},{3,2},{4,5},{5,4},{6,7},{7,6},{8,9},{9,8},{10,11... | collective-permute-start | bytes 442376 | tf_op jit(solution)/shard_map/ppermute | solution.py:621
  132.9 15.6 %collective-permute-start.36 = (bf16[96,768]{1,0:T(8,128)(2,1)S(1)}, bf16[96,768]{1,0:T(8,128)(2,1)S(1)}, u32[]{:S(2)}, u32[]{:S(2)}) collective-permute-start(bf16[96,768]{1,0:T(8,128)(2,1)S(1)} %get-tuple-element.154), channel_id=1, source_target_pairs={{0,8},{1,9},{2,10},{3,11},{4,12},{5,13},{6,14},{7,15},{8,0},{9,1},... | collective-permute-start | bytes 442376 | tf_op jit(solution)/shard_map/ppermute | solution.py:621
  134.1 15.4 %collective-permute-start.38 = (bf16[96,768]{1,0:T(8,128)(2,1)S(1)}, bf16[96,768]{1,0:T(8,128)(2,1)S(1)}, u32[]{:S(2)}, u32[]{:S(2)}) collective-permute-start(bf16[96,768]{1,0:T(8,128)(2,1)S(1)} %get-tuple-element.157), channel_id=1, source_target_pairs={{0,9},{1,8},{2,11},{3,10},{4,13},{5,12},{6,15},{7,14},{8,1},{9,0},... | collective-permute-start | bytes 442376 | tf_op jit(solution)/shard_map/ppermute | solution.py:621
  134.7 16.2 %collective-permute-start.29 = (bf16[96,768]{1,0:T(8,128)(2,1)S(1)}, bf16[96,768]{1,0:T(8,128)(2,1)S(1)}, u32[]{:S(2)}, u32[]{:S(2)}) collective-permute-start(bf16[96,768]{1,0:T(8,128)(2,1)S(1)} %get-tuple-element.145), channel_id=1, source_target_pairs={{0,1},{1,0},{2,3},{3,2},{4,5},{5,4},{6,7},{7,6},{8,9},{9,8},{10,11... | collective-permute-start | bytes 442376 | tf_op jit(solution)/shard_map/ppermute | solution.py:621
  135.1 20.2 %collective-permute-start.40 = (bf16[96,768]{1,0:T(8,128)(2,1)S(1)}, bf16[96,768]{1,0:T(8,128)(2,1)S(1)}, u32[]{:S(2)}, u32[]{:S(2)}) collective-permute-start(bf16[96,768]{1,0:T(8,128)(2,1)S(1)} %get-tuple-element.160), channel_id=1, source_target_pairs={{0,16},{1,17},{2,18},{3,19},{4,20},{5,21},{6,22},{7,23},{8,24},{9,... | collective-permute-start | bytes 442376 | tf_op jit(solution)/shard_map/ppermute | solution.py:621
  149.6 11.7 %collective-permute-start.47 = (bf16[96,768]{1,0:T(8,128)(2,1)S(1)}, bf16[96,768]{1,0:T(8,128)(2,1)S(1)}, u32[]{:S(2)}, u32[]{:S(2)}) collective-permute-start(bf16[96,768]{1,0:T(8,128)(2,1)S(1)} %get-tuple-element.169), channel_id=1, source_target_pairs={{0,24},{1,25},{2,26},{3,27},{4,28},{5,29},{6,30},{7,31},{8,16},{9,... | collective-permute-start | bytes 442376 | tf_op jit(solution)/shard_map/ppermute | solution.py:621
  151.0 11.7 %collective-permute-start.49 = (bf16[96,768]{1,0:T(8,128)(2,1)S(1)}, bf16[96,768]{1,0:T(8,128)(2,1)S(1)}, u32[]{:S(2)}, u32[]{:S(2)}) collective-permute-start(bf16[96,768]{1,0:T(8,128)(2,1)S(1)} %get-tuple-element.172), channel_id=1, source_target_pairs={{0,25},{1,24},{2,27},{3,26},{4,29},{5,28},{6,31},{7,30},{8,17},{9,... | collective-permute-start | bytes 442376 | tf_op jit(solution)/shard_map/ppermute | solution.py:621
  157.3 11.5 %collective-permute-start.37 = (bf16[96,768]{1,0:T(8,128)(2,1)S(1)}, bf16[96,768]{1,0:T(8,128)(2,1)S(1)}, u32[]{:S(2)}, u32[]{:S(2)}) collective-permute-start(bf16[96,768]{1,0:T(8,128)(2,1)S(1)} %get-tuple-element.156), channel_id=1, source_target_pairs={{0,9},{1,8},{2,11},{3,10},{4,13},{5,12},{6,15},{7,14},{8,1},{9,0},... | collective-permute-start | bytes 442376 | tf_op jit(solution)/shard_map/ppermute | solution.py:621
  162.7 16.5 %collective-permute-start.41 = (bf16[96,768]{1,0:T(8,128)(2,1)S(1)}, bf16[96,768]{1,0:T(8,128)(2,1)S(1)}, u32[]{:S(2)}, u32[]{:S(2)}) collective-permute-start(bf16[96,768]{1,0:T(8,128)(2,1)S(1)} %get-tuple-element.162), channel_id=1, source_target_pairs={{0,17},{1,16},{2,19},{3,18},{4,21},{5,20},{6,23},{7,22},{8,25},{9,... | collective-permute-start | bytes 442376 | tf_op jit(solution)/shard_map/ppermute | solution.py:621
  166.6 17.6 %collective-permute-start.56 = (bf16[96,768]{1,0:T(8,128)(2,1)S(1)}, bf16[96,768]{1,0:T(8,128)(2,1)S(1)}, u32[]{:S(2)}, u32[]{:S(2)}) collective-permute-start(bf16[96,768]{1,0:T(8,128)(2,1)S(1)} %get-tuple-element.182), channel_id=1, source_target_pairs={{0,1},{1,0},{2,3},{3,2},{4,5},{5,4},{6,7},{7,6},{8,9},{9,8},{10,11... | collective-permute-start | bytes 442376 | tf_op jit(solution)/shard_map/ppermute | solution.py:621
  167.3 18.6 %collective-permute-start.34 = (bf16[96,768]{1,0:T(8,128)(2,1)S(1)}, bf16[96,768]{1,0:T(8,128)(2,1)S(1)}, u32[]{:S(2)}, u32[]{:S(2)}) collective-permute-start(bf16[96,768]{1,0:T(8,128)(2,1)S(1)} %get-tuple-element.152), channel_id=1, source_target_pairs={{0,1},{1,0},{2,3},{3,2},{4,5},{5,4},{6,7},{7,6},{8,9},{9,8},{10,11... | collective-permute-start | bytes 442376 | tf_op jit(solution)/shard_map/ppermute | solution.py:621
  168.8 19.2 %collective-permute-start.61 = (bf16[96,768]{1,0:T(8,128)(2,1)S(1)}, bf16[96,768]{1,0:T(8,128)(2,1)S(1)}, u32[]{:S(2)}, u32[]{:S(2)}) collective-permute-start(bf16[96,768]{1,0:T(8,128)(2,1)S(1)} %get-tuple-element.187), channel_id=1, source_target_pairs={{0,24},{1,25},{2,26},{3,27},{4,28},{5,29},{6,30},{7,31},{8,16},{9,... | collective-permute-start | bytes 442376 | tf_op jit(solution)/shard_map/ppermute | solution.py:621
  170.5 18.9 %collective-permute-start.62 = (bf16[96,768]{1,0:T(8,128)(2,1)S(1)}, bf16[96,768]{1,0:T(8,128)(2,1)S(1)}, u32[]{:S(2)}, u32[]{:S(2)}) collective-permute-start(bf16[96,768]{1,0:T(8,128)(2,1)S(1)} %get-tuple-element.188), channel_id=1, source_target_pairs={{0,25},{1,24},{2,27},{3,26},{4,29},{5,28},{6,31},{7,30},{8,17},{9,... | collective-permute-start | bytes 442376 | tf_op jit(solution)/shard_map/ppermute | solution.py:621
  189.4 12.2 %collective-permute-start.66 = (bf16[192,512]{1,0:T(8,128)(2,1)S(1)}, bf16[192,512]{1,0:T(8,128)(2,1)S(1)}, u32[]{:S(2)}, u32[]{:S(2)}) collective-permute-start(bf16[192,512]{1,0:T(8,128)(2,1)S(1)} %get-tuple-element.202), channel_id=1, source_target_pairs={{0,2},{1,3},{2,4},{3,5},{4,6},{5,7},{6,0},{7,1},{8,10},{9,11},{10,... | collective-permute-start | bytes 589832 | tf_op jit(solution)/shard_map/ppermute | solution.py:613
  189.5 17.2 %collective-permute-start.67 = (bf16[192,512]{1,0:T(8,128)(2,1)S(1)}, bf16[192,512]{1,0:T(8,128)(2,1)S(1)}, u32[]{:S(2)}, u32[]{:S(2)}) collective-permute-start(bf16[192,512]{1,0:T(8,128)(2,1)S(1)} %get-tuple-element.203), channel_id=1, source_target_pairs={{0,4},{1,5},{2,6},{3,7},{4,0},{5,1},{6,2},{7,3},{8,12},{9,13},{10,... | collective-permute-start | bytes 589832 | tf_op jit(solution)/shard_map/ppermute | solution.py:613
  208.8 15.4 %collective-permute-start.63 = (bf16[64,768]{1,0:T(8,128)(2,1)S(1)}, bf16[64,768]{1,0:T(8,128)(2,1)S(1)}, u32[]{:S(2)}, u32[]{:S(2)}) collective-permute-start(bf16[64,768]{1,0:T(8,128)(2,1)S(1)} %get-tuple-element.190), channel_id=1, source_target_pairs={{0,2},{1,3},{2,4},{3,5},{4,6},{5,7},{6,0},{7,1},{8,10},{9,11},{10,... | collective-permute-start | bytes 294920 | tf_op jit(solution)/shard_map/ppermute | solution.py:613
  223.0 12.5 %collective-permute-start.54 = (bf16[64,768]{1,0:T(8,128)(2,1)S(1)}, bf16[64,768]{1,0:T(8,128)(2,1)S(1)}, u32[]{:S(2)}, u32[]{:S(2)}) collective-permute-start(bf16[64,768]{1,0:T(8,128)(2,1)S(1)} %get-tuple-element.179), channel_id=1, source_target_pairs={{0,4},{1,5},{2,6},{3,7},{4,0},{5,1},{6,2},{7,3},{8,12},{9,13},{10,... | collective-permute-start | bytes 294920 | tf_op jit(solution)/shard_map/ppermute | solution.py:613
  (71 other events, 560.9 us)

commit v2 on v1

--- a/solution.py
+++ b/solution.py
@@ -75,32 +75,12 @@
     meta_ref[...] = meta
 
 
-def early_kernel(
-    raw_hbm, speed_hbm, fade_hbm, *refs,
-):
-    count = (len(refs) - 7) // 2
-    in_refs, out_refs = refs[:count], refs[count : 2 * count]
-    rows_ref, cols_ref, totals_ref, raw_ref, speed_ref, fade_ref, sems = refs[2 * count :]
-    pairs = [(raw_hbm, raw_ref), (speed_hbm, speed_ref), (fade_hbm, fade_ref)]
-    pairs += list(zip(in_refs, out_refs))
-    copies = [pltpu.make_async_copy(a, b, sems.at[n]) for n, (a, b) in enumerate(pairs)]
-    for copy in copies:
-        copy.start()
-    for copy in copies[:3]:
-        copy.wait()
-    heads, steps = raw_ref.shape[1:]
+def early_kernel(step_ref, decay_ref, rows_ref, cols_ref, totals_ref):
+    heads, steps = step_ref.shape[1:]
     lane = lax.broadcasted_iota(jnp.int32, (heads, steps), 1)
-    eye = lax.broadcasted_iota(jnp.int32, (heads, heads), 0) == lax.broadcasted_iota(
-        jnp.int32, (heads, heads), 1
-    )
     sums, weights = [], []
     for d in range(2):
-        raw = raw_ref[d].astype(F32)
-        step = jnp.maximum(raw, 0.0) + jnp.log1p(jnp.exp(-jnp.abs(raw)))
-        speed = jnp.sum(
-            jnp.where(eye, jnp.exp(speed_ref[d : d + 1, :]), 0.0), axis=1, keepdims=True
-        )
-        run = -step * speed + fade_ref[d]
+        step, run = step_ref[d], decay_ref[d]
         shift = 1
         while shift < steps:
             if d == 0:
@@ -117,43 +97,38 @@
         sums + weights + [jnp.zeros((STATE - 4 * heads, steps), F32)], axis=0
     )
     cols_ref[...] = stacked.T
-    for copy in copies[3:]:
-        copy.wait()
 
 
 def prepare_kernel(
-    x_ref, b_ref, c_ref, low_ref, high_ref, tx_ref, tb_ref, tc_ref, cols_ref, totals_ref,
+    all_ref, low_ref, high_ref, taps_ref, cols_ref, totals_ref,
     xc_ref, bc_ref, cc_ref, *rest, axis,
 ):
     *msg_refs, pad_ref = rest
-    steps = x_ref.shape[0]
+    steps = all_ref.shape[0]
     heads = totals_ref.shape[1]
-    groups = b_ref.shape[1] // STATE
+    groups = bc_ref.shape[1] // STATE
     per_group = heads // groups
     wide = per_group * HEAD_DIM
     here = lax.axis_index(axis)
     cols = cols_ref[...]
     totals = [totals_ref[d, :, 0:1] for d in range(2)]
 
-    def conv(ref, taps_ref, at, start):
-        pad_ref[PAD - 2 : PAD] = low_ref[:, at + start : at + start + TILE].astype(F32)
-        pad_ref[PAD : PAD + steps] = ref[:, start : start + TILE].astype(F32)
-        pad_ref[PAD + steps : PAD + steps + 2] = high_ref[
-            :, at + start : at + start + TILE
-        ].astype(F32)
-        taps = taps_ref[:, start : start + TILE].astype(F32)
+    def conv(start):
+        lanes = slice(start, start + TILE)
+        pad_ref[PAD - 2 : PAD] = low_ref[:, lanes].astype(F32)
+        pad_ref[PAD : PAD + steps] = all_ref[:, lanes].astype(F32)
+        pad_ref[PAD + steps : PAD + steps + 2] = high_ref[:, lanes].astype(F32)
+        taps = taps_ref[:, lanes].astype(F32)
         total = taps[0:1] * pad_ref[PAD - 2 : PAD - 2 + steps]
         for j in range(1, taps.shape[0]):
             total = total + taps[j : j + 1] * pad_ref[PAD - 2 + j : PAD - 2 + j + steps]
         return silu(total)
 
     at = 0
-    for ref, taps_ref, out_ref in (
-        (x_ref, tx_ref, xc_ref), (b_ref, tb_ref, bc_ref), (c_ref, tc_ref, cc_ref),
-    ):
-        for start in range(0, ref.shape[1], TILE):
-            out_ref[:, start : start + TILE] = conv(ref, taps_ref, at, start).astype(BF16)
-        at += ref.shape[1]
+    for out_ref in (xc_ref, bc_ref, cc_ref):
+        for start in range(0, out_ref.shape[1], TILE):
+            out_ref[:, start : start + TILE] = conv(at + start).astype(BF16)
+        at += out_ref.shape[1]
 
     row = lax.broadcasted_iota(jnp.int32, (EXTRA, wide), 0)
     own = lax.broadcasted_iota(jnp.int32, (per_group, wide), 0) == (
@@ -307,12 +282,19 @@
     last = jnp.concatenate([x[-rim:], b[-rim:], c[-rim:]], axis=1)
     low = lax.ppermute(last, "sp", [(i, i + 1) for i in range(count - 1)])
     high = lax.ppermute(first, "sp", [(i + 1, i) for i in range(count - 1)])
-    x, b, c, tx, tb, tc, rows, cols, totals = early(x, b, c, tx, tb, tc)
+    rows, cols, totals = early()
     heads = rows.shape[1]
     message = jax.ShapeDtypeStruct((groups, STATE + EXTRA, wide), BF16)
     xc, bc, cc, *sends = kernel(
         functools.partial(prepare_kernel, axis="sp"),
-        (x, b, c, low, high, tx, tb, tc, cols, totals),
+        (
+            jnp.concatenate([x, b, c], axis=1),
+            low,
+            high,
+            jnp.concatenate([tx, tb, tc], axis=1),
+            cols,
+            totals,
+        ),
         [jax.ShapeDtypeStruct(v.shape, BF16) for v in (x, b, c)] + [message] * (count - 1),
         scratch_shapes=[pltpu.VMEM((steps + 2 * PAD, TILE), F32)],
     )
@@ -624,20 +606,17 @@
     widths = chunk_widths(width)
     slim = [jax.ShapeDtypeStruct((rows, columns), BF16) for columns in widths]
 
-    def early(*inputs):
-        small = (raw_increments, channel_log_fade_speed, extra_log_fade)
+    def early():
+        step = jax.nn.softplus(raw_increments.astype(F32))
+        decay = extra_log_fade - step * jnp.exp(channel_log_fade_speed)[..., None]
         return kernel(
             early_kernel,
-            (*small, *inputs),
-            [jax.ShapeDtypeStruct(v.shape, v.dtype) for v in inputs]
-            + [
+            (step, decay),
+            [
                 jax.ShapeDtypeStruct(raw_increments.shape, F32),
                 jax.ShapeDtypeStruct((raw_increments.shape[2], STATE), F32),
                 jax.ShapeDtypeStruct((*raw_increments.shape[:2], STATE), F32),
             ],
-            in_specs=[pl.BlockSpec(memory_space=pltpu.HBM)] * (len(small) + len(inputs)),
-            scratch_shapes=[pltpu.VMEM(v.shape, v.dtype) for v in small]
-            + [pltpu.SemaphoreType.DMA((len(small) + len(inputs),))],
         )
 
     keep, send = mixer(

time: 237 us -> 232 us (0.979)
  local copies, waits for them, and re-layouts: 15.4 us -> 8.94 us
  waiting for transfers between devices: 93.6 us -> 90.1 us
  other arithmetic: 0.01 us -> 2.98 us
  starting transfers between devices: 95.2 us -> 97.8 us
    unnamed x40 -> x22, local copies, waits for them, and re-layouts: 13.9 us -> 6.79 us
    ppermute x3, starting transfers between devices: 11 us -> 5.09 us  [mixer(): lax.ppermute(send, 'sp', [(i, i ^ k) for i in range(count)])]
    ppermute x24, waiting for transfers between devices: 56.8 us -> 50.9 us  [to_chip(): return lax.ppermute(value, 'tp', pairs)]
    ppermute x24, starting transfers between devices: 39 us -> 44.7 us  [to_chip(): return lax.ppermute(value, 'tp', pairs)]
    ppermute x42, starting transfers between devices: 38 us -> 40.7 us  [to_peer(): return lax.ppermute(value, ('sp', 'tp'), pairs)]
    ppermute x1, waiting for transfers between devices: 0.01 us -> 2.71 us  [mixer(): high = lax.ppermute(first, 'sp', [(i + 1, i) for i in range(count - 1)])]
    ppermute x3, waiting for transfers between devices: 6.25 us -> 8.72 us  [mixer(): lax.ppermute(send, 'sp', [(i, i ^ k) for i in range(count)])]
  transfers between devices with their start and end apart: 76 -> 76, of which waited for: 32 -> 32; matrix products, arithmetic and copies ran while one was open for 1% -> 2% of each run, Pallas kernels for 13% -> 13%
where the time goes in v2:
time: 232 us; the launch traced here: 231 us
  starting transfers between devices  97.8 us (42%)
  waiting for transfers between devices  90.1 us (39%)
  Pallas kernels  31 us (13%)
  local copies, waits for them, and re-layouts  8.94 us (4%)
  other arithmetic  2.98 us (1%)
    ppermute x24, waiting for transfers between devices, to_chip(): return lax.ppermute(value, 'tp', pairs)  50.9 us
    ppermute x24, starting transfers between devices, to_chip(): return lax.ppermute(value, 'tp', pairs)  44.7 us
    ppermute x42, starting transfers between devices, to_peer(): return lax.ppermute(value, ('sp', 'tp'), pairs)  40.7 us
    pallas_call x31, Pallas kernels, kernel(): pl.pallas_call(body, out_shape=outs, out_specs=vmem(len(outs)) if isinsta...  31 us
    ppermute x42, waiting for transfers between devices, to_peer(): return lax.ppermute(value, ('sp', 'tp'), pairs)  26.2 us
    ppermute x3, waiting for transfers between devices, mixer(): lax.ppermute(send, 'sp', [(i, i ^ k) for i in range(count)])  8.72 us
    unnamed x22, local copies, waits for them, and re-layouts  6.79 us
    ppermute x3, starting transfers between devices, mixer(): lax.ppermute(send, 'sp', [(i, i ^ k) for i in range(count)])  5.09 us
  transfers between devices with their start and end apart: 76, of which 32 were waited for; matrix products, arithmetic and copies ran while one was open for 2% of the time, Pallas kernels for 13%

profile of v2, /device:TPU:0, one launch (start us, length us, event | category | flops | bytes accessed | tf_op | source)
XLA Modules:
  0.0 231.3 jit_solution(5487445757115192811)
XLA Ops:
  2.5 4.9 %collective-permute-start = (bf16[2,1024]{1,0:T(2,128)(2,1)S(1)}, bf16[2,1024]{1,0:T(2,128)(2,1)S(1)}, u32[]{:S(2)}, u32[]{:S(2)}) collective-permute-start(bf16[2,1024]{1,0:T(2,128)(2,1)S(1)} %pad_maximum_fusion.2), channel_id=1, source_target_pairs={{0,8},{8,16},{16,24},{1,9},{9,17},{17,25},{2,10},{10,18},{18,26},{... | collective-permute-start | bytes 12296 | tf_op jit(solution)/shard_map/ppermute | solution.py:283
  15.8 3.1 %shard_map.182 = (bf16[512,512]{1,0:T(8,128)(2,1)S(1)}, bf16[512,256]{1,0:T(8,128)(2,1)S(1)}, bf16[512,256]{1,0:T(8,128)(2,1)S(1)}, bf16[2,144,256]{2,1,0:T(8,12...) custom-call(bf16[512,1024]{1,0:T(8,128)(2,1)S(1)} %pad_maximum_fusion.all_ref, ...), custom_call_target="tpu_custom_call" | custom-call | tf_op jit(solution)/shard_map/pallas_call | solution.py:261
  21.4 3.1 %collective-permute-done.2.rest_0_ = bf16[2,144,256]{2,1,0:T(8,128)(2,1)S(1)} collective-permute-done((bf16[2,144,256]{2,1,0:T(8,128)(2,1)S(1)}, bf16[2,144,256]{2,1,0:T(8,128)(2,1)S(1)}, u32[]{:S(2)}, u32[]{:S(2)}) %collective-permute-start.2) | collective-permute-done | bytes 147488 | tf_op jit(solution)/shard_map/ppermute | solution.py:302
  25.7 4.0 %collective-permute-done.3.rest_1_ = bf16[2,144,256]{2,1,0:T(8,128)(2,1)S(1)} collective-permute-done((bf16[2,144,256]{2,1,0:T(8,128)(2,1)S(1)}, bf16[2,144,256]{2,1,0:T(8,128)(2,1)S(1)}, u32[]{:S(2)}, u32[]{:S(2)}) %collective-permute-start.3) | collective-permute-done | bytes 147488 | tf_op jit(solution)/shard_map/ppermute | solution.py:302
  31.1 2.9 %shard_map.183.y_ref = f32[512,512]{1,0:T(8,128)S(1)} custom-call(bf16[512,512]{1,0:T(8,128)(2,1)S(1)} %get-tuple-element.105.xc_ref, bf16[512,256]{1,0:T(8,128)(2,1)S(1)} %get-tuple-element.106.bc_ref, bf16[512,256]{1,0:T(8,128)(2,1)S(1)} %get-tuple-element.107.cc_ref, f32[2,8,512]{2,1,0:T(8,128)S(1)} %get-tuple-element.108.rows_ref, ...), custom_call_target="tpu_custom_call" | custom-call | flops 1610612736 | bytes 2097152 | tf_op jit(solution)/shard_map/pallas_call | solution.py:261
  45.2 6.5 %collective-permute-done.12.refs_3_ = f32[64,128]{1,0:T(8,128)S(1)} collective-permute-done((f32[64,128]{1,0:T(8,128)S(1)}, f32[64,128]{1,0:T(8,128)S(1)}, u32[]{:S(2)}, u32[]{:S(2)}) %collective-permute-start.12) | collective-permute-done | bytes 32800 | tf_op jit(solution)/shard_map/ppermute | solution.py:595
  54.6 11.9 %collective-permute-done.8.refs_2_ = bf16[64,2048]{1,0:T(8,128)(2,1)S(1)} collective-permute-done((bf16[64,2048]{1,0:T(8,128)(2,1)S(1)}, bf16[64,2048]{1,0:T(8,128)(2,1)S(1)}, u32[]{:S(2)}, u32[]{:S(2)}) %collective-permute-start.8) | collective-permute-done | bytes 262176 | tf_op jit(solution)/shard_map/ppermute | solution.py:595
  66.5 7.3 %collective-permute-start.10 = (f32[64,128]{1,0:T(8,128)S(1)}, f32[64,128]{1,0:T(8,128)S(1)}, u32[]{:S(2)}, u32[]{:S(2)}) collective-permute-start(f32[64,128]{1,0:T(8,128)S(1)} %shard_map.187.refs_0_.meta_ref), channel_id=1, source_target_pairs={{0,2},{1,3},{2,4},{3,5},{4,6},{5,7},{6,0},{7,1},{8,10},{9,11},{10,... | collective-permute-start | bytes 98312 | tf_op jit(solution)/shard_map/ppermute | solution.py:595
  75.5 3.6 %collective-permute-start.20 = (bf16[24,512]{1,0:T(8,128)(2,1)S(1)}, bf16[24,512]{1,0:T(8,128)(2,1)S(1)}, u32[]{:S(2)}, u32[]{:S(2)}) collective-permute-start(bf16[24,512]{1,0:T(8,128)(2,1)S(1)} %get-tuple-element.126), channel_id=1, source_target_pairs={{0,8},{1,9},{2,10},{3,11},{4,12},{5,13},{6,14},{7,15},{8,0},{9,1},... | collective-permute-start | bytes 73736 | tf_op jit(solution)/shard_map/ppermute | solution.py:603
  86.2 3.3 %collective-permute-done.24.refs_6_ = bf16[24,512]{1,0:T(8,128)(2,1)S(1)} collective-permute-done((bf16[24,512]{1,0:T(8,128)(2,1)S(1)}, bf16[24,512]{1,0:T(8,128)(2,1)S(1)}, u32[]{:S(2)}, u32[]{:S(2)}) %collective-permute-start.24) | collective-permute-done | bytes 24608 | tf_op jit(solution)/shard_map/ppermute | solution.py:603
  95.3 4.2 %collective-permute-start.13 = (bf16[64,768]{1,0:T(8,128)(2,1)S(1)}, bf16[64,768]{1,0:T(8,128)(2,1)S(1)}, u32[]{:S(2)}, u32[]{:S(2)}) collective-permute-start(bf16[64,768]{1,0:T(8,128)(2,1)S(1)} %get-tuple-element.119.refs_4_), channel_id=1, source_target_pairs={{0,2},{1,3},{2,4},{3,5},{4,6},{5,7},{6,0},{7,1},{8,10},{9,11},{10,... | collective-permute-start | bytes 294920 | tf_op jit(solution)/shard_map/ppermute | solution.py:595
  103.6 3.2 %collective-permute-done.18.refs_7_ = bf16[64,768]{1,0:T(8,128)(2,1)S(1)} collective-permute-done((bf16[64,768]{1,0:T(8,128)(2,1)S(1)}, bf16[64,768]{1,0:T(8,128)(2,1)S(1)}, u32[]{:S(2)}, u32[]{:S(2)}) %collective-permute-start.18) | collective-permute-done | bytes 98336 | tf_op jit(solution)/shard_map/ppermute | solution.py:595
  111.3 4.2 %collective-permute-done.16.refs_5_ = bf16[64,768]{1,0:T(8,128)(2,1)S(1)} collective-permute-done((bf16[64,768]{1,0:T(8,128)(2,1)S(1)}, bf16[64,768]{1,0:T(8,128)(2,1)S(1)}, u32[]{:S(2)}, u32[]{:S(2)}) %collective-permute-start.16) | collective-permute-done | bytes 98336 | tf_op jit(solution)/shard_map/ppermute | solution.py:595
  119.2 9.0 %collective-permute-done.27.refs_2_ = bf16[192,512]{1,0:T(8,128)(2,1)S(1)} collective-permute-done((bf16[192,512]{1,0:T(8,128)(2,1)S(1)}, bf16[192,512]{1,0:T(8,128)(2,1)S(1)}, u32[]{:S(2)}, u32[]{:S(2)}) %collective-permute-start.27) | collective-permute-done | bytes 196640 | tf_op jit(solution)/shard_map/ppermute | solution.py:595
  138.1 3.4 %shard_map.193 = (bf16[4,2048,256]{2,1,0:T(8,128)(2,1)S(1)}, bf16[4,2048,256]{2,1,0:T(8,128)(2,1)S(1)}, bf16[1024,2048]{1,0:T(8,128)(2,1)S(1)}) custom-call(bf16[2,2048,512]{2,1,0:T(8,128)(2,1)S(1)} %copy-done, bf16[2,2048,512]{2,1,0:T(8,128)(2,1)S(1)} %copy-done.1, bf16[2,512,2048]{2,1,0:T(8,128)(2,1)S(1)} %copy-done.2, ...), custom_call_target="tpu_custom_call" | custom-call | tf_op jit(solution)/shard_map/pallas_call | solution.py:261
  141.5 3.2 %collective-permute-start.48 = (bf16[96,768]{1,0:T(8,128)(2,1)S(1)}, bf16[96,768]{1,0:T(8,128)(2,1)S(1)}, u32[]{:S(2)}, u32[]{:S(2)}) collective-permute-start(bf16[96,768]{1,0:T(8,128)(2,1)S(1)} %get-tuple-element.158), channel_id=1, source_target_pairs={{0,24},{1,25},{2,26},{3,27},{4,28},{5,29},{6,30},{7,31},{8,16},{9,... | collective-permute-start | bytes 442376 | tf_op jit(solution)/shard_map/ppermute | solution.py:603
  166.9 6.1 %collective-permute-done.41.refs_9_ = bf16[96,768]{1,0:T(8,128)(2,1)S(1)} collective-permute-done((bf16[96,768]{1,0:T(8,128)(2,1)S(1)}, bf16[96,768]{1,0:T(8,128)(2,1)S(1)}, u32[]{:S(2)}, u32[]{:S(2)}) %collective-permute-start.41) | collective-permute-done | bytes 147488 | tf_op jit(solution)/shard_map/ppermute | solution.py:603
  173.0 3.5 %collective-permute-start.51 = (bf16[96,768]{1,0:T(8,128)(2,1)S(1)}, bf16[96,768]{1,0:T(8,128)(2,1)S(1)}, u32[]{:S(2)}, u32[]{:S(2)}) collective-permute-start(bf16[96,768]{1,0:T(8,128)(2,1)S(1)} %get-tuple-element.163), channel_id=1, source_target_pairs={{0,24},{1,25},{2,26},{3,27},{4,28},{5,29},{6,30},{7,31},{8,16},{9,... | collective-permute-start | bytes 442376 | tf_op jit(solution)/shard_map/ppermute | solution.py:603
  176.5 3.4 %shard_map.196.hidden_ref = bf16[384,1024]{1,0:T(8,128)(2,1)S(1)} custom-call(bf16[96,768]{1,0:T(8,128)(2,1)S(1)} %collective-permute-done.35.refs_0_, bf16[96,768]{1,0:T(8,128)(2,1)S(1)} %collective-permute-done.36.refs_1_, bf16[96,512]{1,0:T(8,128)(2,1)S(1)} %get-tuple-element.143.refs_2_, bf16[96,768]{1,0:T(8,128)(2,1)S(1)} %collective-permute-done.37.refs_3_, ...), custom_call_target="tpu_custom_call" | custom-call | flops 3221225472 | bytes 8388608 | tf_op jit(solution)/shard_map/pallas_call | solution.py:261
  184.6 3.3 %collective-permute-done.52.refs_11_ = bf16[96,768]{1,0:T(8,128)(2,1)S(1)} collective-permute-done((bf16[96,768]{1,0:T(8,128)(2,1)S(1)}, bf16[96,768]{1,0:T(8,128)(2,1)S(1)}, u32[]{:S(2)}, u32[]{:S(2)}) %collective-permute-start.52) | collective-permute-done | bytes 147488 | tf_op jit(solution)/shard_map/ppermute | solution.py:603
  197.8 3.3 %collective-permute-done.67.refs_2_ = bf16[192,512]{1,0:T(8,128)(2,1)S(1)} collective-permute-done((bf16[192,512]{1,0:T(8,128)(2,1)S(1)}, bf16[192,512]{1,0:T(8,128)(2,1)S(1)}, u32[]{:S(2)}, u32[]{:S(2)}) %collective-permute-start.67) | collective-permute-done | bytes 196640 | tf_op jit(solution)/shard_map/ppermute | solution.py:595
  202.3 3.4 %collective-permute-start.63 = (bf16[64,768]{1,0:T(8,128)(2,1)S(1)}, bf16[64,768]{1,0:T(8,128)(2,1)S(1)}, u32[]{:S(2)}, u32[]{:S(2)}) collective-permute-start(bf16[64,768]{1,0:T(8,128)(2,1)S(1)} %get-tuple-element.178), channel_id=1, source_target_pairs={{0,2},{1,3},{2,4},{3,5},{4,6},{5,7},{6,0},{7,1},{8,10},{9,11},{10,... | collective-permute-start | bytes 294920 | tf_op jit(solution)/shard_map/ppermute | solution.py:595
  219.5 2.9 %collective-permute-start.55 = (bf16[64,768]{1,0:T(8,128)(2,1)S(1)}, bf16[64,768]{1,0:T(8,128)(2,1)S(1)}, u32[]{:S(2)}, u32[]{:S(2)}) collective-permute-start(bf16[64,768]{1,0:T(8,128)(2,1)S(1)} %get-tuple-element.168), channel_id=1, source_target_pairs={{0,6},{1,7},{2,0},{3,1},{4,2},{5,3},{6,4},{7,5},{8,14},{9,15},{10,... | collective-permute-start | bytes 294920 | tf_op jit(solution)/shard_map/ppermute | solution.py:595
  225.4 5.1 %collective-permute-done.54.refs_2_ = bf16[64,768]{1,0:T(8,128)(2,1)S(1)} collective-permute-done((bf16[64,768]{1,0:T(8,128)(2,1)S(1)}, bf16[64,768]{1,0:T(8,128)(2,1)S(1)}, u32[]{:S(2)}, u32[]{:S(2)}) %collective-permute-start.54) | collective-permute-done | bytes 98336 | tf_op jit(solution)/shard_map/ppermute | solution.py:595
  (189 shorter events, 122.2 us)
Async XLA Ops:
  0.0 130.9 %collective-permute-start.31 = (bf16[2,2048,512]{2,1,0:T(8,128)(2,1)}, bf16[2,2048,512]{2,1,0:T(8,128)(2,1)}, u32[]{:S(2)}, u32[]{:S(2)}) collective-permute-start(bf16[2,2048,512]{2,1,0:T(8,128)(2,1)} %refs_0_.1), channel_id=1, source_target_pairs={{0,1},{1,0},{2,3},{3,2},{4,5},{5,4},{6,7},{7,6},{8,9},{9,8},{10,11... | collective-permute-start | bytes 12582920 | tf_op jit(solution)/shard_map/ppermute | solution.py:591
  0.5 130.6 %collective-permute-start.32 = (bf16[2,2048,512]{2,1,0:T(8,128)(2,1)}, bf16[2,2048,512]{2,1,0:T(8,128)(2,1)}, u32[]{:S(2)}, u32[]{:S(2)}) collective-permute-start(bf16[2,2048,512]{2,1,0:T(8,128)(2,1)} %refs_1_.1), channel_id=1, source_target_pairs={{0,1},{1,0},{2,3},{3,2},{4,5},{5,4},{6,7},{7,6},{8,9},{9,8},{10,11... | collective-permute-start | bytes 12582920 | tf_op jit(solution)/shard_map/ppermute | solution.py:591
  0.5 130.8 %collective-permute-start.33 = (bf16[2,512,2048]{2,1,0:T(8,128)(2,1)}, bf16[2,512,2048]{2,1,0:T(8,128)(2,1)}, u32[]{:S(2)}, u32[]{:S(2)}) collective-permute-start(bf16[2,512,2048]{2,1,0:T(8,128)(2,1)} %refs_2_.1), channel_id=1, source_target_pairs={{0,1},{1,0},{2,3},{3,2},{4,5},{5,4},{6,7},{7,6},{8,9},{9,8},{10,11... | collective-permute-start | bytes 12582920 | tf_op jit(solution)/shard_map/ppermute | solution.py:591
  1.0 38.4 %collective-permute-start.6 = (bf16[512,2048]{1,0:T(8,128)(2,1)}, bf16[512,2048]{1,0:T(8,128)(2,1)S(1)}, u32[]{:S(2)}, u32[]{:S(2)}) collective-permute-start(bf16[512,2048]{1,0:T(8,128)(2,1)} %own_w_ref.1), channel_id=1, source_target_pairs={{0,1},{1,0},{2,3},{3,2},{4,5},{5,4},{6,7},{7,6},{8,9},{9,8},{10,11... | collective-permute-start | bytes 6291464 | tf_op jit(solution)/shard_map/ppermute | solution.py:591
  40.7 11.6 %collective-permute-start.7 = (bf16[64,2048]{1,0:T(8,128)(2,1)S(1)}, bf16[64,2048]{1,0:T(8,128)(2,1)S(1)}, u32[]{:S(2)}, u32[]{:S(2)}) collective-permute-start(bf16[64,2048]{1,0:T(8,128)(2,1)S(1)} %get-tuple-element.115), channel_id=1, source_target_pairs={{0,2},{1,3},{2,4},{3,5},{4,6},{5,7},{6,0},{7,1},{8,10},{9,11},{10,... | collective-permute-start | bytes 786440 | tf_op jit(solution)/shard_map/ppermute | solution.py:595
  51.7 14.8 %collective-permute-start.8 = (bf16[64,2048]{1,0:T(8,128)(2,1)S(1)}, bf16[64,2048]{1,0:T(8,128)(2,1)S(1)}, u32[]{:S(2)}, u32[]{:S(2)}) collective-permute-start(bf16[64,2048]{1,0:T(8,128)(2,1)S(1)} %get-tuple-element.116), channel_id=1, source_target_pairs={{0,4},{1,5},{2,6},{3,7},{4,0},{5,1},{6,2},{7,3},{8,12},{9,13},{10,... | collective-permute-start | bytes 786440 | tf_op jit(solution)/shard_map/ppermute | solution.py:595
  52.3 14.2 %collective-permute-start.9 = (bf16[64,2048]{1,0:T(8,128)(2,1)S(1)}, bf16[64,2048]{1,0:T(8,128)(2,1)S(1)}, u32[]{:S(2)}, u32[]{:S(2)}) collective-permute-start(bf16[64,2048]{1,0:T(8,128)(2,1)S(1)} %get-tuple-element.117), channel_id=1, source_target_pairs={{0,6},{1,7},{2,0},{3,1},{4,2},{5,3},{6,4},{7,5},{8,14},{9,15},{10,... | collective-permute-start | bytes 786440 | tf_op jit(solution)/shard_map/ppermute | solution.py:595
  115.5 12.7 %collective-permute-start.27 = (bf16[192,512]{1,0:T(8,128)(2,1)S(1)}, bf16[192,512]{1,0:T(8,128)(2,1)S(1)}, u32[]{:S(2)}, u32[]{:S(2)}) collective-permute-start(bf16[192,512]{1,0:T(8,128)(2,1)S(1)} %shard_map.191.refs_0_), channel_id=1, source_target_pairs={{0,4},{1,5},{2,6},{3,7},{4,0},{5,1},{6,2},{7,3},{8,12},{9,13},{10,... | collective-permute-start | bytes 589832 | tf_op jit(solution)/shard_map/ppermute | solution.py:595
  128.3 13.2 %collective-permute-start.30 = (bf16[96,768]{1,0:T(8,128)(2,1)S(1)}, bf16[96,768]{1,0:T(8,128)(2,1)S(1)}, u32[]{:S(2)}, u32[]{:S(2)}) collective-permute-start(bf16[96,768]{1,0:T(8,128)(2,1)S(1)} %get-tuple-element.134), channel_id=1, source_target_pairs={{0,1},{1,0},{2,3},{3,2},{4,5},{5,4},{6,7},{7,6},{8,9},{9,8},{10,11... | collective-permute-start | bytes 442376 | tf_op jit(solution)/shard_map/ppermute | solution.py:603
  128.3 16.4 %collective-permute-start.36 = (bf16[96,768]{1,0:T(8,128)(2,1)S(1)}, bf16[96,768]{1,0:T(8,128)(2,1)S(1)}, u32[]{:S(2)}, u32[]{:S(2)}) collective-permute-start(bf16[96,768]{1,0:T(8,128)(2,1)S(1)} %get-tuple-element.142), channel_id=1, source_target_pairs={{0,8},{1,9},{2,10},{3,11},{4,12},{5,13},{6,14},{7,15},{8,0},{9,1},... | collective-permute-start | bytes 442376 | tf_op jit(solution)/shard_map/ppermute | solution.py:603
  130.9 13.8 %collective-permute-start.38 = (bf16[96,768]{1,0:T(8,128)(2,1)S(1)}, bf16[96,768]{1,0:T(8,128)(2,1)S(1)}, u32[]{:S(2)}, u32[]{:S(2)}) collective-permute-start(bf16[96,768]{1,0:T(8,128)(2,1)S(1)} %get-tuple-element.145), channel_id=1, source_target_pairs={{0,9},{1,8},{2,11},{3,10},{4,13},{5,12},{6,15},{7,14},{8,1},{9,0},... | collective-permute-start | bytes 442376 | tf_op jit(solution)/shard_map/ppermute | solution.py:603
  131.1 15.8 %collective-permute-start.29 = (bf16[96,768]{1,0:T(8,128)(2,1)S(1)}, bf16[96,768]{1,0:T(8,128)(2,1)S(1)}, u32[]{:S(2)}, u32[]{:S(2)}) collective-permute-start(bf16[96,768]{1,0:T(8,128)(2,1)S(1)} %get-tuple-element.133), channel_id=1, source_target_pairs={{0,1},{1,0},{2,3},{3,2},{4,5},{5,4},{6,7},{7,6},{8,9},{9,8},{10,11... | collective-permute-start | bytes 442376 | tf_op jit(solution)/shard_map/ppermute | solution.py:603
  131.3 18.9 %collective-permute-start.40 = (bf16[96,768]{1,0:T(8,128)(2,1)S(1)}, bf16[96,768]{1,0:T(8,128)(2,1)S(1)}, u32[]{:S(2)}, u32[]{:S(2)}) collective-permute-start(bf16[96,768]{1,0:T(8,128)(2,1)S(1)} %get-tuple-element.148), channel_id=1, source_target_pairs={{0,16},{1,17},{2,18},{3,19},{4,20},{5,21},{6,22},{7,23},{8,24},{9,... | collective-permute-start | bytes 442376 | tf_op jit(solution)/shard_map/ppermute | solution.py:603
  146.9 11.6 %collective-permute-start.49 = (bf16[96,768]{1,0:T(8,128)(2,1)S(1)}, bf16[96,768]{1,0:T(8,128)(2,1)S(1)}, u32[]{:S(2)}, u32[]{:S(2)}) collective-permute-start(bf16[96,768]{1,0:T(8,128)(2,1)S(1)} %get-tuple-element.160), channel_id=1, source_target_pairs={{0,25},{1,24},{2,27},{3,26},{4,29},{5,28},{6,31},{7,30},{8,17},{9,... | collective-permute-start | bytes 442376 | tf_op jit(solution)/shard_map/ppermute | solution.py:603
  150.2 12.5 %collective-permute-start.42 = (bf16[96,768]{1,0:T(8,128)(2,1)S(1)}, bf16[96,768]{1,0:T(8,128)(2,1)S(1)}, u32[]{:S(2)}, u32[]{:S(2)}) collective-permute-start(bf16[96,768]{1,0:T(8,128)(2,1)S(1)} %get-tuple-element.151), channel_id=1, source_target_pairs={{0,17},{1,16},{2,19},{3,18},{4,21},{5,20},{6,23},{7,22},{8,25},{9,... | collective-permute-start | bytes 442376 | tf_op jit(solution)/shard_map/ppermute | solution.py:603
  158.4 14.6 %collective-permute-start.41 = (bf16[96,768]{1,0:T(8,128)(2,1)S(1)}, bf16[96,768]{1,0:T(8,128)(2,1)S(1)}, u32[]{:S(2)}, u32[]{:S(2)}) collective-permute-start(bf16[96,768]{1,0:T(8,128)(2,1)S(1)} %get-tuple-element.150), channel_id=1, source_target_pairs={{0,17},{1,16},{2,19},{3,18},{4,21},{5,20},{6,23},{7,22},{8,25},{9,... | collective-permute-start | bytes 442376 | tf_op jit(solution)/shard_map/ppermute | solution.py:603
  162.8 18.0 %collective-permute-start.56 = (bf16[96,768]{1,0:T(8,128)(2,1)S(1)}, bf16[96,768]{1,0:T(8,128)(2,1)S(1)}, u32[]{:S(2)}, u32[]{:S(2)}) collective-permute-start(bf16[96,768]{1,0:T(8,128)(2,1)S(1)} %get-tuple-element.170), channel_id=1, source_target_pairs={{0,1},{1,0},{2,3},{3,2},{4,5},{5,4},{6,7},{7,6},{8,9},{9,8},{10,11... | collective-permute-start | bytes 442376 | tf_op jit(solution)/shard_map/ppermute | solution.py:603
  162.8 18.0 %collective-permute-start.34 = (bf16[96,768]{1,0:T(8,128)(2,1)S(1)}, bf16[96,768]{1,0:T(8,128)(2,1)S(1)}, u32[]{:S(2)}, u32[]{:S(2)}) collective-permute-start(bf16[96,768]{1,0:T(8,128)(2,1)S(1)} %get-tuple-element.140), channel_id=1, source_target_pairs={{0,1},{1,0},{2,3},{3,2},{4,5},{5,4},{6,7},{7,6},{8,9},{9,8},{10,11... | collective-permute-start | bytes 442376 | tf_op jit(solution)/shard_map/ppermute | solution.py:603
  163.7 17.9 %collective-permute-start.61 = (bf16[96,768]{1,0:T(8,128)(2,1)S(1)}, bf16[96,768]{1,0:T(8,128)(2,1)S(1)}, u32[]{:S(2)}, u32[]{:S(2)}) collective-permute-start(bf16[96,768]{1,0:T(8,128)(2,1)S(1)} %get-tuple-element.175), channel_id=1, source_target_pairs={{0,24},{1,25},{2,26},{3,27},{4,28},{5,29},{6,30},{7,31},{8,16},{9,... | collective-permute-start | bytes 442376 | tf_op jit(solution)/shard_map/ppermute | solution.py:603
  165.2 18.6 %collective-permute-start.62 = (bf16[96,768]{1,0:T(8,128)(2,1)S(1)}, bf16[96,768]{1,0:T(8,128)(2,1)S(1)}, u32[]{:S(2)}, u32[]{:S(2)}) collective-permute-start(bf16[96,768]{1,0:T(8,128)(2,1)S(1)} %get-tuple-element.176), channel_id=1, source_target_pairs={{0,25},{1,24},{2,27},{3,26},{4,29},{5,28},{6,31},{7,30},{8,17},{9,... | collective-permute-start | bytes 442376 | tf_op jit(solution)/shard_map/ppermute | solution.py:603
  183.8 13.1 %collective-permute-start.66 = (bf16[192,512]{1,0:T(8,128)(2,1)S(1)}, bf16[192,512]{1,0:T(8,128)(2,1)S(1)}, u32[]{:S(2)}, u32[]{:S(2)}) collective-permute-start(bf16[192,512]{1,0:T(8,128)(2,1)S(1)} %get-tuple-element.190), channel_id=1, source_target_pairs={{0,2},{1,3},{2,4},{3,5},{4,6},{5,7},{6,0},{7,1},{8,10},{9,11},{10,... | collective-permute-start | bytes 589832 | tf_op jit(solution)/shard_map/ppermute | solution.py:595
  183.9 17.2 %collective-permute-start.67 = (bf16[192,512]{1,0:T(8,128)(2,1)S(1)}, bf16[192,512]{1,0:T(8,128)(2,1)S(1)}, u32[]{:S(2)}, u32[]{:S(2)}) collective-permute-start(bf16[192,512]{1,0:T(8,128)(2,1)S(1)} %get-tuple-element.191), channel_id=1, source_target_pairs={{0,4},{1,5},{2,6},{3,7},{4,0},{5,1},{6,2},{7,3},{8,12},{9,13},{10,... | collective-permute-start | bytes 589832 | tf_op jit(solution)/shard_map/ppermute | solution.py:595
  202.3 17.2 %collective-permute-start.63 = (bf16[64,768]{1,0:T(8,128)(2,1)S(1)}, bf16[64,768]{1,0:T(8,128)(2,1)S(1)}, u32[]{:S(2)}, u32[]{:S(2)}) collective-permute-start(bf16[64,768]{1,0:T(8,128)(2,1)S(1)} %get-tuple-element.178), channel_id=1, source_target_pairs={{0,2},{1,3},{2,4},{3,5},{4,6},{5,7},{6,0},{7,1},{8,10},{9,11},{10,... | collective-permute-start | bytes 294920 | tf_op jit(solution)/shard_map/ppermute | solution.py:595
  218.0 12.4 %collective-permute-start.54 = (bf16[64,768]{1,0:T(8,128)(2,1)S(1)}, bf16[64,768]{1,0:T(8,128)(2,1)S(1)}, u32[]{:S(2)}, u32[]{:S(2)}) collective-permute-start(bf16[64,768]{1,0:T(8,128)(2,1)S(1)} %get-tuple-element.167), channel_id=1, source_target_pairs={{0,4},{1,5},{2,6},{3,7},{4,0},{5,1},{6,2},{7,3},{8,12},{9,13},{10,... | collective-permute-start | bytes 294920 | tf_op jit(solution)/shard_map/ppermute | solution.py:595
  (62 other events, 549.3 us)
